TPU v7x, 32 devices: a whole 2x2x4 slice. The times are simulated.
32 devices in a mesh: sp: 4 (over y, core), tp: 8 (over z, x).
Axes of the slice: x: 2, y: 2, z: 4, core: 2. Of those that a mesh axis runs over, the one named last changes fastest.
Arguments:
- queries: bfloat16 [512, 3072], P('sp'), may hold values from -6 to 6
- attn_out: bfloat16 [512, 3072], P('sp'), may hold values from -3 to 3
- log_norm: float32 [512, 12], P('sp'), as said below
- cotangent: bfloat16 [512, 3072], P('sp'), may hold values from -96 to 96
- keys: bfloat16 [1024, 512], P(('sp', 'tp')), may hold values from -6 to 6
- values: bfloat16 [1024, 512], P(('sp', 'tp')), may hold values from -6 to 6
- source: bfloat16 [1024, 3072], P('sp', 'tp'), may hold values from -6 to 6
- w_query: bfloat16 [3072, 3072], P('tp'), may hold values from -0.109375 to 0.109375
- w_key: bfloat16 [3072, 512], P('tp'), may hold values from -0.109375 to 0.109375
- w_value: bfloat16 [3072, 512], P('tp'), may hold values from -0.109375 to 0.109375
Outputs:
- d_target: bfloat16 [512, 3072], P('sp', 'tp')
- d_source: bfloat16 [1024, 3072], P('sp', 'tp')
- d_wvalue: float32 [3072, 512], P('tp')
Inputs may be any that keep to these rules, and one draw needn't show every extreme that they name: `log_norm`: the logarithm of the softmax total saved by the forward pass, near log(1024) + 0.5.
All inputs are finite; a program needn't handle non-finite values.
Results may differ from a plain program's by a relative error of at most 0.024.
Values may be sent and summed in bfloat16 or wider, within the bound.
A program may use at most 64 MiB of HBM per device.

v0:
```python
import functools
import math

import jax
import jax.numpy as jnp
from jax import lax
from jax.experimental import pallas as pl
from jax.experimental.pallas import tpu as pltpu
from jax.sharding import PartitionSpec as P

HEADS = 12
KV_HEADS = 2
HEAD_DIM = 256
CORES = 2
SIDE = 2
VMEM_BYTES = 60 * 1024 * 1024
MESH = pl.DeviceIdType.MESH
NT = (((1,), (1,)), ((), ()))
TN = (((0,), (0,)), ((), ()))
F32 = jnp.float32
BF16 = jnp.bfloat16


def dot(a, b, dims=(((1,), (0,)), ((), ()))):
    return lax.dot_general(a, b, dims, preferred_element_type=F32)


def kernel(
    sp, tp, lse_ref, k_ref, v_ref, q_hbm, o_hbm, do_hbm, src_hbm, wq_hbm, wk_hbm, wv_hbm,
    dt_hbm, ds_hbm, dw_hbm,
    dt_ref, ds_ref, dw_ref, kv, qs, dos, os_, wq, wk, wv, src, src_t, lse, delta, dqa, dq16, part, got, full,
    load_sem, near_send, near_recv, kv_send, kv_recv, kv_pair_send, kv_pair_recv,
    src_send, src_recv, part_send, part_recv, g_send, g_recv, gy_send, gy_recv, gp_send, gp_recv, kvz_send, gz_send,
):
    rows = q_hbm.shape[0]
    rs, kw = k_ref.shape
    repeat = HEADS // KV_HEADS
    scale = 1.0 / math.sqrt(HEAD_DIM)
    i, j = lax.axis_index("sp"), lax.axis_index("tp")
    ny, nz = sp // CORES, tp // SIDE
    y, c = i // CORES, lax.rem(i, CORES)
    z, x = j // SIDE, lax.rem(j, SIDE)
    sp_peers = [lax.rem(i + k, sp) for k in range(1, sp)]
    y_peers = [lax.rem(y + k, ny) * CORES + c for k in range(1, ny)]
    pair = y * CORES + 1 - c
    orders = [sorted((b for b in range(nz) if b != a), key=lambda b, a=a: abs(a - b)) for a in range(nz)]
    zs = [sum(jnp.where(z == a, order[n], 0) for a, order in enumerate(orders)) for n in range(nz - 1)]
    onward = [jnp.where(a > z, z - 1, z + 1) for a in zs]
    onward_ok = [(b >= 0) & (b < nz) for b in onward]
    z_peers = [a * SIDE + x for a in zs]
    jx = z * SIDE + 1 - x
    sends = []
    maybe_sends = []

    def send_if(condition, make):
        pl.when(condition)(lambda: make().start())
        maybe_sends.append((condition, make))

    def along_z(ref, n, s, r):
        targets = [(z + 1, z + 1 < nz, 0), (z - 1, z >= 1, 1)] if n is None else [(onward[n], onward_ok[n], n + 2)]
        for to, ok, at in targets:
            send_if(ok, lambda to=to, at=at: pltpu.make_async_remote_copy(
                src_ref=ref, dst_ref=ref, send_sem=s.at[at], recv_sem=r,
                device_id=(i, to * SIDE + x), device_id_type=MESH,
            ))

    def send(ref_from, ref_to, s, r, device):
        copy = pltpu.make_async_remote_copy(
            src_ref=ref_from, dst_ref=ref_to, send_sem=s, recv_sem=r,
            device_id=device, device_id_type=MESH,
        )
        copy.start()
        sends.append(copy)

    def receive(ref, r):
        pltpu.make_async_remote_copy(
            src_ref=ref, dst_ref=ref, send_sem=load_sem.at[0], recv_sem=r,
            device_id=(pair, j), device_id_type=MESH,
        ).wait_recv()

    loads = []

    def load(ref_from, ref_to):
        copy = pltpu.make_async_copy(ref_from, ref_to, load_sem.at[len(loads)])
        copy.start()
        loads.append(copy)
        return copy

    barrier = pltpu.get_barrier_semaphore()
    near = [(p, j) for p in sp_peers] + [(i, p) for p in z_peers] + [(i, jx)]
    for d in near:
        pl.semaphore_signal(barrier, inc=1, device_id=d, device_id_type=MESH)
    near_rows = pl.ds(pl.multiple_of(i * rs, rs), rs)
    own_copies = [load(r, kv.at[t, j, near_rows]) for t, r in enumerate((k_ref, v_ref))]
    attn_loads = []
    for g in range(KV_HEADS):
        for h in range(repeat):
            columns = pl.ds((g * repeat + h) * HEAD_DIM, HEAD_DIM)
            for a, b in ((q_hbm, qs), (do_hbm, dos), (o_hbm, os_)):
                attn_loads.append(load(a.at[:, columns], b.at[g, pl.ds(h * rows, rows)]))
    src_load = load(src_hbm, src.at[i])
    weight_loads = [load(wq_hbm, wq), load(wk_hbm, wk), load(wv_hbm, wv)]
    pl.semaphore_wait(barrier, len(near))

    for n, p in enumerate(sp_peers):
        for t, r in enumerate((k_ref, v_ref)):
            send(r, kv.at[t, j, near_rows], near_send.at[t, n], near_recv.at[t, i], (p, j))

    for copy in attn_loads:
        copy.wait()
    for g in range(KV_HEADS):
        for h in range(repeat):
            at = pl.ds(h * rows, rows)
            d = jnp.sum(dos[g, at].astype(F32) * os_[g, at].astype(F32), axis=1, keepdims=True)
            delta[g, at] = jnp.broadcast_to(d, (rows, 128))
            n = g * repeat + h
            lse[g, at] = jnp.transpose(jnp.broadcast_to(lse_ref[n:n + 1, :], (128, rows)))

    for copy in own_copies:
        copy.wait()
    for p in sp_peers:
        for t in range(2):
            receive(kv.at[t, j, pl.ds(pl.multiple_of(p * rs, rs), rs)], near_recv.at[t, p])

    def kv_to_x(slot, n):
        send(kv.at[c, slot], kv.at[c, slot], kv_send.at[n], kv_recv.at[slot], (i, jx))

    def kv_to_pair(slot):
        send(kv.at[c, slot], kv.at[c, slot], kv_pair_send.at[slot], kv_pair_recv.at[slot], (pair, j))

    kv_to_x(j, 0)
    along_z(kv.at[c, j], None, kvz_send, kv_recv.at[j])

    def wide(a, n):
        return a if n == 1 else jnp.concatenate([a] * n, axis=1)

    def grads(g, keys, values):
        n = keys.shape[0] // 128
        p = jnp.exp(dot(qs[g], keys, NT) * scale - wide(lse[g], n))
        dp = dot(dos[g], values, NT)
        ds = (p * (dp - wide(delta[g], n))).astype(BF16)
        return p, ds

    def head_columns(g):
        return slice(g * HEAD_DIM, (g + 1) * HEAD_DIM)

    for g in range(KV_HEADS):
        cols = head_columns(g)
        keys = kv[0, j, :, cols]
        p, ds = grads(g, keys, kv[1, j, :, cols])
        dk = dot(ds, qs[g], TN) * scale
        dv = dot(p.astype(BF16), dos[g], TN)
        part[:, 0, :, cols] = dk.astype(BF16).reshape(sp, rs, HEAD_DIM)
        part[:, 1, :, cols] = dv.astype(BF16).reshape(sp, rs, HEAD_DIM)
        dqa[g] = dot(ds, keys)
    for n, p in enumerate(sp_peers):
        send(part.at[p], got.at[i], part_send.at[n], part_recv.at[i], (p, j))
    src_load.wait()
    for n, p in enumerate(y_peers):
        send(src.at[i], src.at[i], src_send.at[n], src_recv.at[i], (p, j))
    send(src.at[i], src.at[i], src_send.at[ny], src_recv.at[i], (pair, j))

    def chunk_one(slot):
        for g in range(KV_HEADS):
            cols = head_columns(g)
            keys = kv[0, slot, :, cols]
            _, ds = grads(g, keys, kv[1, slot, :, cols])
            dqa[g] += dot(ds, keys)

    def chunk_z(a):
        slots = pl.ds(a * SIDE, SIDE)
        for g in range(KV_HEADS):
            cols = head_columns(g)
            keys = kv[0, slots, :, cols].reshape(-1, HEAD_DIM)
            values = kv[1, slots, :, cols].reshape(-1, HEAD_DIM)
            _, ds = grads(g, keys, values)
            dqa[g] += dot(ds, keys)

    def from_z(n):
        slot = z_peers[n]
        receive(kv.at[c, slot], kv_recv.at[slot])
        along_z(kv.at[c, slot], n, kvz_send, kv_recv.at[slot])
        kv_to_x(slot, n + 1)
        kv_to_pair(slot)

    def from_x(slot):
        receive(kv.at[c, slot], kv_recv.at[slot])
        kv_to_pair(slot)

    def from_pair(slot):
        receive(kv.at[1 - c, slot], kv_pair_recv.at[slot])

    def g_to_x(slot, n):
        send(full.at[i, slot], full.at[i, slot], g_send.at[n], g_recv.at[slot], (i, jx))

    def g_spread(slot):
        for n, p in enumerate(y_peers):
            send(full.at[i, slot, 1], full.at[i, slot, 1], gy_send.at[n, slot], gy_recv.at[i, slot], (p, j))
        send(full.at[i, slot, 1], full.at[i, slot, 1], gp_send.at[i, slot], gp_recv.at[i, slot], (pair, j))

    def g_from_z(n):
        slot = z_peers[n]
        receive(full.at[i, slot], g_recv.at[slot])
        along_z(full.at[i, slot], n, gz_send, g_recv.at[slot])
        g_to_x(slot, n + 1)
        g_spread(slot)

    def g_from_x(slot):
        receive(full.at[i, slot], g_recv.at[slot])
        g_spread(slot)

    def g_from_y(slot):
        for p in y_peers:
            receive(full.at[p, slot, 1], gy_recv.at[p, slot])
            send(full.at[p, slot, 1], full.at[p, slot, 1], gp_send.at[p, slot], gp_recv.at[p, slot], (pair, j))

    far = [a * SIDE + 1 - x for a in zs]
    from_x(jx)
    from_z(0)
    total = part[i].astype(F32)
    for p in sp_peers:
        receive(got.at[p], part_recv.at[p])
        total += got[p].astype(F32)
    full[i, j] = total.astype(BF16)
    along_z(full.at[i, j], None, gz_send, g_recv.at[j])
    g_to_x(j, 0)
    g_spread(j)
    from_pair(jx)
    chunk_one(jx)
    for n in range(nz - 1):
        if n + 1 < nz - 1:
            from_z(n + 1)
        from_x(far[n])
        g_from_z(n)
        if n == 0:
            g_from_x(jx)
            for m, p in enumerate(y_peers):
                receive(src.at[p], src_recv.at[p])
                send(src.at[p], src.at[p], src_send.at[ny + 1 + m], src_recv.at[p], (pair, j))
        else:
            g_from_x(far[n - 1])
        g_from_y([j, jx, z_peers[0]][n])
        from_pair(z_peers[n])
        from_pair(far[n])
        chunk_z(zs[n])
    g_from_x(far[nz - 2])
    for copy in weight_loads:
        copy.wait()
    for g in range(KV_HEADS):
        for h in range(repeat):
            n = g * repeat + h
            dq16[:, n * HEAD_DIM:(n + 1) * HEAD_DIM] = (dqa[g, h * rows:(h + 1) * rows] * scale).astype(BF16)
    theirs = [lax.rem(y + k, ny) * CORES + 1 - c for k in range(ny)]
    for p in theirs:
        receive(src.at[p], src_recv.at[p])
    for b in range(sp):
        src_t[b] = jnp.transpose(src[b])
    dt_ref[...] = dot(dq16[...], wq[...], NT).astype(BF16)
    results = [load(dt_ref, dt_hbm)]
    for slot in z_peers[1:] + far:
        g_from_y(slot)
    ds_ref[...] = (
        dot(full[i, :, 0].reshape(-1, kw), wk[...], NT) + dot(full[i, :, 1].reshape(-1, kw), wv[...], NT)
    ).astype(BF16)
    results.append(load(ds_ref, ds_hbm))
    for p in theirs:
        for slot in range(tp):
            receive(full.at[p, slot, 1], gp_recv.at[p, slot])
    dw = dot(src_t[0], full[0, :, 1].reshape(-1, kw))
    for b in range(1, sp):
        dw += dot(src_t[b], full[b, :, 1].reshape(-1, kw))
    dw_ref[...] = dw
    results.append(load(dw_ref, dw_hbm))
    for copy in results:
        copy.wait()
    for copy in sends:
        copy.wait_send()
    for condition, make in maybe_sends:
        pl.when(condition)(lambda make=make: make().wait_send())


def settle(*refs):
    count = (len(refs) - 1) // 3
    sems = refs[-1]
    ins, outs, held = (refs[n * count:(n + 1) * count] for n in range(3))
    steps = []
    for n in range(count):
        tall = ins[n].shape[0]
        pieces = 4 if n == count - 1 and tall % 32 == 0 else 1
        for m in range(pieces):
            at = pl.ds(m * (tall // pieces), tall // pieces)
            k = len(steps)
            steps.append((
                pltpu.make_async_copy(ins[n].at[at], held[n].at[at], sems.at[0, k]),
                pltpu.make_async_copy(held[n].at[at], outs[n].at[at], sems.at[1, k]),
            ))
    for arrive, _ in steps:
        arrive.start()
    for arrive, leave in steps:
        arrive.wait()
        leave.start()
    for _, leave in steps:
        leave.wait()


def settled(arrays):
    hbm = pl.BlockSpec(memory_space=pl.ANY)
    return pl.pallas_call(
        settle,
        out_shape=tuple(jax.ShapeDtypeStruct(a.shape, a.dtype) for a in arrays),
        in_specs=[hbm] * len(arrays),
        out_specs=(hbm,) * len(arrays),
        scratch_shapes=[pltpu.VMEM(a.shape, a.dtype) for a in arrays] + [
            pltpu.SemaphoreType.DMA((2, len(arrays) + 3))
        ],
        compiler_params=pltpu.CompilerParams(vmem_limit_bytes=VMEM_BYTES),
    )(*arrays)


def fused(sp, tp, scratch, queries, attn_out, log_norm, cotangent, keys, values, source, w_query, w_key, w_value):
    rows = queries.shape[0]
    width = w_value.shape[0]
    vmem, hbm = pl.BlockSpec(memory_space=pltpu.VMEM), pl.BlockSpec(memory_space=pl.ANY)
    dma = pltpu.SemaphoreType.DMA
    nz, ny = tp // SIDE, sp // CORES
    return settled(pl.pallas_call(
        functools.partial(kernel, sp, tp),
        out_shape=(
            jax.ShapeDtypeStruct((rows, width), BF16),
            jax.ShapeDtypeStruct((source.shape[0], width), BF16),
            jax.ShapeDtypeStruct(w_value.shape, F32),
        ),
        in_specs=[vmem] * 3 + [hbm] * 7,
        out_specs=(hbm,) * 3,
        scratch_shapes=[
            pltpu.VMEM((rows, width), BF16), pltpu.VMEM((source.shape[0], width), BF16), pltpu.VMEM(w_value.shape, F32),
        ] + [pltpu.VMEM(s, t) for s, t in scratch] + [
            dma((3 * HEADS + 9,)), dma((2, sp)), dma((2, sp)), dma((2 * nz,)), dma((tp,)), dma((tp,)), dma((tp,)),
            dma((2 * ny,)), dma((sp,)), dma((sp,)), dma((sp,)), dma((2 * nz,)), dma((tp,)),
            dma((ny, tp)), dma((sp, tp)), dma((sp, tp)), dma((sp, tp)), dma((nz + 1,)), dma((nz + 1,)),
        ],
        compiler_params=pltpu.CompilerParams(
            collective_id=0, has_side_effects=True, vmem_limit_bytes=VMEM_BYTES
        ),
    )(log_norm.T, keys, values, queries, attn_out, cotangent, source, w_query, w_key, w_value))


def scratch_of(sp, tp, queries, keys, source, w_query, w_value):
    rows, width = queries.shape
    rs, kw = keys.shape
    stack = (KV_HEADS, rows * HEADS // KV_HEADS, HEAD_DIM)
    flat = stack[:2] + (128,)
    return [
        ((2, tp, sp * rs, kw), BF16), (stack, BF16), (stack, BF16), (stack, BF16),
        (w_query.shape, BF16), (w_value.shape, BF16), (w_value.shape, BF16),
        ((sp,) + source.shape, BF16), ((sp,) + source.shape[::-1], BF16), (flat, F32), (flat, F32), (stack, F32), ((rows, width), BF16),
        ((sp, 2, rs, kw), BF16), ((sp, 2, rs, kw), BF16), ((sp, tp, 2, rs, kw), BF16),
    ]


def shards(sp, tp, *args):
    queries, _, _, _, keys, _, source, w_query, _, w_value = args
    scratch = scratch_of(sp, tp, queries, keys, source, w_query, w_value)
    size = sum(math.prod(s) * jnp.dtype(t).itemsize for s, t in scratch)
    fits = size * 2 < VMEM_BYTES and sp * keys.shape[0] == 128
    if fits and sp % CORES == 0 and tp == 4 * SIDE:
        return fused(sp, tp, scratch, *args)
    return plain(*args)


def plain(queries, attn_out, log_norm, cotangent, keys, values, source, w_query, w_key, w_value):
    single_precision = jnp.float32
    repeat = HEADS // KV_HEADS
    score_scale = 1.0 / math.sqrt(HEAD_DIM)
    rows = queries.shape[0]
    near_keys, near_values = (
        lax.all_gather(keys, "sp", axis=0, tiled=True),
        lax.all_gather(values, "sp", axis=0, tiled=True),
    )
    span = near_keys.shape[0]
    query_tensor4 = queries.reshape(rows, KV_HEADS, repeat, HEAD_DIM)
    output_gradient4 = cotangent.reshape(rows, KV_HEADS, repeat, HEAD_DIM)
    out4 = attn_out.reshape(rows, KV_HEADS, repeat, HEAD_DIM)
    shared_key_heads = near_keys.reshape(span, KV_HEADS, HEAD_DIM)
    shared_value_heads = near_values.reshape(span, KV_HEADS, HEAD_DIM)
    delta = jnp.sum(
        output_gradient4.astype(single_precision) * out4.astype(single_precision), axis=3
    )
    delta = jnp.transpose(delta, (1, 2, 0))[..., None]
    lse = jnp.transpose(log_norm.reshape(rows, KV_HEADS, repeat), (1, 2, 0))[..., None]
    logit_scores = (
        jnp.einsum(
            "znjk,wnk->njzw",
            query_tensor4,
            shared_key_heads,
            preferred_element_type=single_precision,
        )
        * score_scale
    )
    probs = jnp.exp(logit_scores - lse)
    probabilities16 = probs.astype(jnp.bfloat16)
    prob_gradient = jnp.einsum(
        "znjk,wnk->njzw",
        output_gradient4,
        shared_value_heads,
        preferred_element_type=single_precision,
    )
    score_gradient = (probs * (prob_gradient - delta)).astype(jnp.bfloat16)
    query_gradient_piece = (
        jnp.einsum(
            "wohn,nwb->hwob",
            score_gradient,
            shared_key_heads,
            preferred_element_type=single_precision,
        )
        * score_scale
    )
    query_gradient_piece = query_gradient_piece.reshape(rows, -1)
    key_gradient_piece = (
        jnp.einsum(
            "nkjv,jnka->vna", score_gradient, query_tensor4, preferred_element_type=single_precision
        )
        * score_scale
    )
    value_gradient_piece = jnp.einsum(
        "nkjv,jnka->vna", probabilities16, output_gradient4, preferred_element_type=single_precision
    )
    own_keys, own_values = (
        lax.psum_scatter(
            key_gradient_piece.reshape(span, -1).astype(jnp.bfloat16),
            "sp",
            scatter_dimension=0,
            tiled=True,
        ).astype(jnp.float32),
        lax.psum_scatter(
            value_gradient_piece.reshape(span, -1).astype(jnp.bfloat16),
            "sp",
            scatter_dimension=0,
            tiled=True,
        ).astype(jnp.float32),
    )
    stacked = jnp.concatenate(
        [own_keys.astype(jnp.bfloat16), own_values.astype(jnp.bfloat16)], axis=1
    )
    group = lax.all_gather(stacked, "tp", axis=0, tiled=True)
    weights = jnp.concatenate([w_key, w_value], axis=1)
    d_source = lax.dot_general(
        group, weights, (((1,), (1,)), ((), ())), preferred_element_type=single_precision
    ).astype(jnp.bfloat16)
    kv_width = w_value.shape[1]
    weight_term = lax.dot_general(
        source,
        group[:, kv_width:],
        (((0,), (0,)), ((), ())),
        preferred_element_type=single_precision,
    )
    d_wvalue = lax.psum(weight_term.astype(jnp.bfloat16), "sp").astype(jnp.float32)
    dq16 = lax.psum(query_gradient_piece, "tp").astype(jnp.bfloat16)
    d_target = lax.dot_general(
        dq16, w_query, (((1,), (1,)), ((), ())), preferred_element_type=single_precision
    ).astype(jnp.bfloat16)
    return (d_target, d_source, d_wvalue)


def solution(mesh):
    body = functools.partial(shards, mesh.shape["sp"], mesh.shape["tp"])
    in_specs = (
        P("sp", None),
        P("sp", None),
        P("sp", None),
        P("sp", None),
        P(("sp", "tp"), None),
        P(("sp", "tp"), None),
        P("sp", "tp"),
        P("tp", None),
        P("tp", None),
        P("tp", None),
    )
    out_specs = (P("sp", "tp"), P("sp", "tp"), P("tp", None))
    return jax.shard_map(body, mesh=mesh, in_specs=in_specs, out_specs=out_specs, check_vma=False)
```

profile of v0, /device:TPU:0, one launch (start us, length us, event | category | flops | bytes accessed | tf_op | source)
XLA Modules:
  0.0 45.9 jit_solution(15166122662577182465)
XLA Ops:
  0.6 43.2 %shard_map.121 = (bf16[128,384]{1,0:T(8,128)(2,1)}, bf16[256,384]{1,0:T(8,128)(2,1)}, f32[384,512]{1,0:T(8,128)}) custom-call(f32[12,128]{1,0:T(8,128)} %bitcast.1, bf16[32,512]{1,0:T(8,128)(2,1)} %k_ref.1, bf16[32,512]{1,0:T(8,128)(2,1)} %v_ref.1, bf16[128,3072]{1,0:T(8,128)(2,1)} %q_hbm.1, bf16[128,3072]{1,0:T(8,128)(2,1)} %o_hbm.1, ...), custom_call_target="tpu_custom_call" | custom-call | tf_op jit(solution)/shard_map/pallas_call | solution.py:326
  43.8 2.1 %shard_map.122 = (bf16[128,384]{1,0:T(8,128)(2,1)}, bf16[256,384]{1,0:T(8,128)(2,1)}, f32[384,512]{1,0:T(8,128)}) custom-call(bf16[128,384]{1,0:T(8,128)(2,1)} %get-tuple-element.6.refs_0_, bf16[256,384]{1,0:T(8,128)(2,1)} %get-tuple-element.7.refs_1_, f32[384,512]{1,0:T(8,128)} %get-tuple-element.8.refs_2_), custom_call_target="tpu_custom_call" | custom-call | tf_op jit(solution)/shard_map/pallas_call | solution.py:308
where the time goes:
time: 46.1 us; the launch traced here: 45.9 us
  Pallas kernels  45.3 us (98%)
  between operations  0.64 us (1%)
    pallas_call x1, Pallas kernels, fused(): pl.pallas_call(functools.partial(kernel, sp, tp), out_shape=(jax.ShapeDty...  43.2 us
    pallas_call x1, Pallas kernels, settled(): pl.pallas_call(settle, out_shape=tuple((jax.ShapeDtypeStruct(a.shape, a.d...  2.11 us

commit v1 on v0

--- a/solution.py
+++ b/solution.py
@@ -27,8 +27,8 @@
 
 def kernel(
     sp, tp, lse_ref, k_ref, v_ref, q_hbm, o_hbm, do_hbm, src_hbm, wq_hbm, wk_hbm, wv_hbm,
-    dt_hbm, ds_hbm, dw_hbm,
-    dt_ref, ds_ref, dw_ref, kv, qs, dos, os_, wq, wk, wv, src, src_t, lse, delta, dqa, dq16, part, got, full,
+    dt_ref, ds_ref, dw_ref,
+    kv, qs, dos, os_, wq, wk, wv, src, src_t, lse, delta, dqa, dq16, part, got, full,
     load_sem, near_send, near_recv, kv_send, kv_recv, kv_pair_send, kv_pair_recv,
     src_send, src_recv, part_send, part_recv, g_send, g_recv, gy_send, gy_recv, gp_send, gp_recv, kvz_send, gz_send,
 ):
@@ -256,13 +256,11 @@
     for b in range(sp):
         src_t[b] = jnp.transpose(src[b])
     dt_ref[...] = dot(dq16[...], wq[...], NT).astype(BF16)
-    results = [load(dt_ref, dt_hbm)]
     for slot in z_peers[1:] + far:
         g_from_y(slot)
     ds_ref[...] = (
         dot(full[i, :, 0].reshape(-1, kw), wk[...], NT) + dot(full[i, :, 1].reshape(-1, kw), wv[...], NT)
     ).astype(BF16)
-    results.append(load(ds_ref, ds_hbm))
     for p in theirs:
         for slot in range(tp):
             receive(full.at[p, slot, 1], gp_recv.at[p, slot])
@@ -270,9 +268,6 @@
     for b in range(1, sp):
         dw += dot(src_t[b], full[b, :, 1].reshape(-1, kw))
     dw_ref[...] = dw
-    results.append(load(dw_ref, dw_hbm))
-    for copy in results:
-        copy.wait()
     for copy in sends:
         copy.wait_send()
     for condition, make in maybe_sends:
@@ -280,67 +275,50 @@
 
 
 def settle(*refs):
-    count = (len(refs) - 1) // 3
+    count = (len(refs) - 1) // 2
     sems = refs[-1]
-    ins, outs, held = (refs[n * count:(n + 1) * count] for n in range(3))
-    steps = []
-    for n in range(count):
-        tall = ins[n].shape[0]
-        pieces = 4 if n == count - 1 and tall % 32 == 0 else 1
-        for m in range(pieces):
-            at = pl.ds(m * (tall // pieces), tall // pieces)
-            k = len(steps)
-            steps.append((
-                pltpu.make_async_copy(ins[n].at[at], held[n].at[at], sems.at[0, k]),
-                pltpu.make_async_copy(held[n].at[at], outs[n].at[at], sems.at[1, k]),
-            ))
-    for arrive, _ in steps:
-        arrive.start()
-    for arrive, leave in steps:
-        arrive.wait()
-        leave.start()
-    for _, leave in steps:
-        leave.wait()
+    copies = [pltpu.make_async_copy(refs[n], refs[count + n], sems.at[n]) for n in range(count)]
+    for copy in copies:
+        copy.start()
+    for copy in copies:
+        copy.wait()
 
 
 def settled(arrays):
     hbm = pl.BlockSpec(memory_space=pl.ANY)
+    vmem = pl.BlockSpec(memory_space=pltpu.VMEM)
     return pl.pallas_call(
         settle,
         out_shape=tuple(jax.ShapeDtypeStruct(a.shape, a.dtype) for a in arrays),
-        in_specs=[hbm] * len(arrays),
+        in_specs=[vmem] * len(arrays),
         out_specs=(hbm,) * len(arrays),
-        scratch_shapes=[pltpu.VMEM(a.shape, a.dtype) for a in arrays] + [
-            pltpu.SemaphoreType.DMA((2, len(arrays) + 3))
-        ],
-        compiler_params=pltpu.CompilerParams(vmem_limit_bytes=VMEM_BYTES),
+        scratch_shapes=[pltpu.SemaphoreType.DMA((len(arrays),))],
+        compiler_params=pltpu.CompilerParams(vmem_limit_bytes=16 * 1024 * 1024),
     )(*arrays)
 
 
 def fused(sp, tp, scratch, queries, attn_out, log_norm, cotangent, keys, values, source, w_query, w_key, w_value):
     rows = queries.shape[0]
     width = w_value.shape[0]
-    vmem, hbm = pl.BlockSpec(memory_space=pltpu.VMEM), pl.BlockSpec(memory_space=pl.ANY)
+    vmem, hbm = pl.BlockSpec(memory_space=pltpu.VMEM), pl.BlockSpec(memory_space=pltpu.HBM)
     dma = pltpu.SemaphoreType.DMA
     nz, ny = tp // SIDE, sp // CORES
     return settled(pl.pallas_call(
         functools.partial(kernel, sp, tp),
         out_shape=(
-            jax.ShapeDtypeStruct((rows, width), BF16),
-            jax.ShapeDtypeStruct((source.shape[0], width), BF16),
-            jax.ShapeDtypeStruct(w_value.shape, F32),
+            pltpu.VMEM((rows, width), BF16),
+            pltpu.VMEM((source.shape[0], width), BF16),
+            pltpu.VMEM(w_value.shape, F32),
         ),
         in_specs=[vmem] * 3 + [hbm] * 7,
-        out_specs=(hbm,) * 3,
-        scratch_shapes=[
-            pltpu.VMEM((rows, width), BF16), pltpu.VMEM((source.shape[0], width), BF16), pltpu.VMEM(w_value.shape, F32),
-        ] + [pltpu.VMEM(s, t) for s, t in scratch] + [
+        out_specs=(vmem,) * 3,
+        scratch_shapes=[pltpu.VMEM(s, t) for s, t in scratch] + [
             dma((3 * HEADS + 9,)), dma((2, sp)), dma((2, sp)), dma((2 * nz,)), dma((tp,)), dma((tp,)), dma((tp,)),
             dma((2 * ny,)), dma((sp,)), dma((sp,)), dma((sp,)), dma((2 * nz,)), dma((tp,)),
             dma((ny, tp)), dma((sp, tp)), dma((sp, tp)), dma((sp, tp)), dma((nz + 1,)), dma((nz + 1,)),
         ],
         compiler_params=pltpu.CompilerParams(
-            collective_id=0, has_side_effects=True, vmem_limit_bytes=VMEM_BYTES
+            collective_id=0, has_side_effects=True, vmem_limit_bytes=62 * 1024 * 1024
         ),
     )(log_norm.T, keys, values, queries, attn_out, cotangent, source, w_query, w_key, w_value))
 

time: 46.1 us -> 44.1 us (0.957)
  Pallas kernels: 45.3 us -> 43.3 us
    pallas_call x1, Pallas kernels: 2.11 us -> 1.01 us  [settled(): pl.pallas_call(settle, out_shape=tuple((jax.ShapeDtypeStruct(a.shape, a.d...]
    pallas_call x1, Pallas kernels: 43.2 us -> 42.3 us  [fused(): pl.pallas_call(functools.partial(kernel, sp, tp), out_shape=(pltpu.VMEM((...]
where the time goes in v1:
time: 44.1 us; the launch traced here: 43.9 us
  Pallas kernels  43.3 us (98%)
  between operations  0.64 us (1%)
    pallas_call x1, Pallas kernels, fused(): pl.pallas_call(functools.partial(kernel, sp, tp), out_shape=(pltpu.VMEM((...  42.3 us
    pallas_call x1, Pallas kernels, settled(): pl.pallas_call(settle, out_shape=tuple((jax.ShapeDtypeStruct(a.shape, a.d...  1.01 us

profile of v1, /device:TPU:0, one launch (start us, length us, event | category | flops | bytes accessed | tf_op | source)
XLA Modules:
  0.0 43.9 jit_solution(11091380404672293162)
XLA Ops:
  0.6 42.3 %shard_map.121 = (bf16[128,384]{1,0:T(8,128)(2,1)S(1)}, bf16[256,384]{1,0:T(8,128)(2,1)S(1)}, f32[384,512]{1,0:T(8,128)S(1)}) custom-call(f32[12,128]{1,0:T(8,128)} %bitcast.1, bf16[32,512]{1,0:T(8,128)(2,1)} %k_ref.1, bf16[32,512]{1,0:T(8,128)(2,1)} %v_ref.1, bf16[128,3072]{1,0:T(8,128)(2,1)} %q_hbm.1, bf16[128,3072]{1,0:T(8,128)(2,1)} %o_hbm.1, ...), custom_call_target="tpu_custom_call" | custom-call | tf_op jit(solution)/shard_map/pallas_call | solution.py:306
  42.9 1.0 %shard_map.122 = (bf16[128,384]{1,0:T(8,128)(2,1)}, bf16[256,384]{1,0:T(8,128)(2,1)}, f32[384,512]{1,0:T(8,128)}) custom-call(bf16[128,384]{1,0:T(8,128)(2,1)S(1)} %get-tuple-element.6.refs_0_, bf16[256,384]{1,0:T(8,128)(2,1)S(1)} %get-tuple-element.7.refs_1_, f32[384,512]{1,0:T(8,128)S(1)} %get-tuple-element.8.refs_2_), custom_call_target="tpu_custom_call" | custom-call | tf_op jit(solution)/shard_map/pallas_call | solution.py:290

commit v2 on v1

v2 whole, which is shorter than its diff:
```python
import functools
import math

import jax
import jax.numpy as jnp
from jax import lax
from jax.experimental import pallas as pl
from jax.experimental.pallas import tpu as pltpu
from jax.sharding import PartitionSpec as P

HEADS = 12
KV_HEADS = 2
HEAD_DIM = 256
CORES = 2
SIDE = 2
VMEM_BYTES = 62 * 1024 * 1024
UNIT = (16, 256)
MESH = pl.DeviceIdType.MESH
NT = (((1,), (1,)), ((), ()))
TN = (((0,), (0,)), ((), ()))
F32 = jnp.float32
BF16 = jnp.bfloat16


def dot(a, b, dims=(((1,), (0,)), ((), ()))):
    return lax.dot_general(a, b, dims, preferred_element_type=F32)


def kernel(
    sp, tp, lse_hbm, k_hbm, v_hbm, q_hbm, o_hbm, do_hbm, src_hbm, wq_hbm, wk_hbm, wv_hbm,
    dt_ref, ds_ref, dw_ref,
    kv, kvs, att, attr, wq, wk, wv, src, src_t, lsev, lse, delta, dqa, dq16, dqs, acc, part, got, full, units,
    load_sem, send_sem, kv_recv, g_recv, gy_recv, one_recv,
):
    rows = q_hbm.shape[0]
    rs, kw = k_hbm.shape
    repeat = HEADS // KV_HEADS
    scale = 1.0 / math.sqrt(HEAD_DIM)
    log2e = math.log2(math.e)
    unit = UNIT[0] * UNIT[1] * 2
    i, j = lax.axis_index("sp"), lax.axis_index("tp")
    nz = tp // SIDE
    y, c = i // CORES, lax.rem(i, CORES)
    z, x = j // SIDE, lax.rem(j, SIDE)
    oy, oc, ox = 1 - y, 1 - c, 1 - x
    orders = [sorted((b for b in range(nz) if b != a), key=lambda b, a=a: abs(a - b)) for a in range(nz)]
    zs = [sum(jnp.where(z == a, order[n], 0) for a, order in enumerate(orders)) for n in range(nz - 1)]
    mid = (z == 1) | (z == 2)
    edge = jnp.where(z == 1, 0, 3)
    jx = z * SIDE + ox
    mine = [a * SIDE + x for a in zs]
    far = [a * SIDE + ox for a in zs]
    at_pair = (y * CORES + oc, j)
    at_y = (oy * CORES + c, j)
    at_x = (i, jx)
    sent = [0, 0]

    def bytes_of(ref):
        return math.prod(ref.shape) * jnp.dtype(ref.dtype).itemsize

    def send(a, b, r, device, s=0):
        pltpu.make_async_remote_copy(
            src_ref=a, dst_ref=b, send_sem=send_sem.at[s], recv_sem=r, device_id=device, device_id_type=MESH,
        ).start()
        if s < 2:
            sent[s] += bytes_of(a)

    def receive(ref, r):
        pltpu.make_async_remote_copy(
            src_ref=ref, dst_ref=ref, send_sem=send_sem.at[0], recv_sem=r, device_id=at_pair, device_id_type=MESH,
        ).wait_recv()

    def load(a, b, s):
        pltpu.make_async_copy(a, b, load_sem.at[s]).start()
        return bytes_of(b)

    def take(size, s):
        ref = units.at[pl.ds(0, size // unit)]
        pltpu.make_async_copy(ref, ref, load_sem.at[s]).wait()

    own = pl.ds(pl.multiple_of(i * rs, rs), rs)
    theirs = pl.ds(pl.multiple_of((y * CORES + oc) * rs, rs), rs)
    kv_size = 0
    for t, r in enumerate((k_hbm, v_hbm)):
        for g in range(KV_HEADS):
            kv_size += load(r.at[:, pl.ds(g * HEAD_DIM, HEAD_DIM)], kvs.at[t, g], 0)
        kv_size += load(r.at[:, pl.ds(pl.multiple_of(c * HEAD_DIM, HEAD_DIM), HEAD_DIM)], kv.at[t, j, own], 0)
    barrier = pltpu.get_barrier_semaphore()

    def signal(device):
        pl.semaphore_signal(barrier, inc=1, device_id=device, device_id_type=MESH)

    near = [at_pair]
    for g in range(CORES):
        near += [(oy * CORES + g, j), (y * CORES + g, jx), (y * CORES + g, mine[0]), (y * CORES + g, mine[1])]
    for d in near:
        signal(d)

    @pl.when(mid)
    def _():
        for g in range(CORES):
            signal((y * CORES + g, mine[2]))

    def load_heads(g, a, r, s):
        size = 0
        for h in range(repeat):
            columns = pl.ds(pl.multiple_of((g * repeat + h) * HEAD_DIM, HEAD_DIM), HEAD_DIM)
            size += load(r.at[:, columns], att.at[a, g, pl.ds(h * rows, rows)], s)
        return size

    attn = (q_hbm, do_hbm, o_hbm)
    head_size = [load_heads(oc, a, r, 1 + a) for a, r in enumerate(attn)][0]
    own_size = sum(load_heads(c, a, r, 4) for a, r in enumerate(attn))
    load(lse_hbm, lsev.at[0], 5)
    src_size = load(src_hbm, src.at[c, y], 6)
    weight_size = load(wk_hbm, wk, 7) + load(wv_hbm, wv, 7)
    half = wq.shape[2]
    for g in range(KV_HEADS):
        weight_size += load(wq_hbm.at[:, pl.ds(g * half, half)], wq.at[g], 7)
    take(kv_size, 0)
    pl.semaphore_wait(barrier, len(near) + 2 * mid.astype(jnp.int32))


    def raw(y_to, slot, s=0):
        for g in range(CORES):
            send(kvs.at[:, g], kv.at[:, j, own], kv_recv.at[j, y], (y_to * CORES + g, slot), s)

    raw(oy, j)
    raw(y, jx)
    raw(y, mine[0])
    raw(y, mine[1])

    @pl.when(mid)
    def _():
        raw(y, mine[2], 1)

    send(kvs.at[:, oc], kv.at[:, j, own], kv_recv.at[j, y], at_pair)
    for a in range(3):
        take(head_size, 1 + a)
        send(att.at[a, oc], attr.at[a], one_recv.at[0], at_pair)
    pltpu.make_async_copy(lse_hbm, lsev.at[0], load_sem.at[5]).wait()
    send(lsev.at[0], lsev.at[1], one_recv.at[1], at_pair, 2)
    take(own_size, 4)

    def block(b, a):
        return att[a, c] if b == 0 else attr[a]

    def statistics(b):
        for h in range(repeat):
            at = pl.ds(h * rows, rows)
            do, o = (att[a, c, at] if b == 0 else attr[a, at] for a in (1, 2))
            d = jnp.sum(do.astype(F32) * o.astype(F32), axis=1, keepdims=True)
            delta[b, at] = jnp.broadcast_to(d, (rows, 128))
            row = jnp.where(c == 0, lsev[b, h:h + 1, :], lsev[b, repeat + h:repeat + h + 1, :])
            lse[b, at] = jnp.transpose(jnp.broadcast_to(row * log2e, (128, rows)))

    statistics(0)

    def piece(slot, h):
        return kv.at[:, slot, pl.ds(pl.multiple_of(h * (CORES * rs), CORES * rs), CORES * rs)]

    def arrived(slot, h):
        receive(piece(slot, h), kv_recv.at[slot, h])

    def relay(slot, h, device, s=0):
        send(piece(slot, h), piece(slot, h), kv_recv.at[slot, h], device, s)

    def from_z(n, h):
        arrived(mine[n], h)
        relay(mine[n], h, at_x)
        if n == nz - 2:
            pl.when(mid)(lambda: relay(mine[n], h, (i, edge * SIDE + x), 1))

    receive(kv.at[:, j, theirs], kv_recv.at[j, y])
    arrived(j, oy)
    relay(j, oy, at_x)
    relay(j, oy, (i, mine[0]))
    relay(j, oy, (i, mine[1]))
    pl.when(mid)(lambda: relay(j, oy, (i, mine[2]), 1))
    from_z(0, y)
    receive(attr, one_recv.at[0])
    receive(lsev.at[1], one_recv.at[1])
    statistics(1)

    def wide(a, n):
        return a if n == 1 else jnp.concatenate([a] * n, axis=1)

    def grads(b, keys, values):
        n = keys.shape[0] // 128
        p = jnp.exp2(dot(block(b, 0), keys, NT) * (scale * log2e) - wide(lse[b], n))
        dp = dot(block(b, 1), values, NT)
        return p, (p * (dp - wide(delta[b], n))).astype(BF16)

    def local(b):
        keys = kv[0, j]
        p, ds = grads(b, keys, kv[1, j])
        dk = dot(ds, block(b, 0), TN)
        dv = dot(p.astype(BF16), block(b, 1), TN)
        dqa[b] = dot(ds, keys)
        if b == 0:
            acc[0] = dk
            acc[1] = dv
        else:
            part[:, 0] = ((acc[0] + dk) * scale).astype(BF16).reshape(sp, rs, HEAD_DIM)
            part[:, 1] = (acc[1] + dv).astype(BF16).reshape(sp, rs, HEAD_DIM)

    local(0)
    from_z(1, y)
    local(1)
    for g in range(CORES):
        to = oy * CORES + g
        send(part.at[to], got.at[1 + c], one_recv.at[2], (to, j))
    send(part.at[y * CORES + oc], got.at[0], one_recv.at[2], at_pair)
    take(src_size, 6)
    for device, r in ((at_y, 3), (at_pair, 4)):
        send(src.at[c, y], src.at[c, y], one_recv.at[r], device)

    def chunk(slots, order=(0, 1)):
        for b in order:
            keys, values = (kv[t, slots].reshape(-1, HEAD_DIM) for t in range(2))
            _, ds = grads(b, keys, values)
            dqa[b] += dot(ds, keys)

    arrived(jx, y)
    arrived(jx, oy)
    chunk(pl.ds(jx, 1))
    from_z(0, oy)
    from_z(1, oy)
    receive(got, one_recv.at[2])
    here = part[i].astype(F32) + got[1 + c].astype(F32)
    there = got[0].astype(F32) + got[1 + oc].astype(F32)
    for g in range(KV_HEADS):
        full[c, y, j, :, :, g * HEAD_DIM:(g + 1) * HEAD_DIM] = jnp.where(c == g, here, there).astype(BF16)

    def g_send(slot, device, only=None, s=0):
        ref = full.at[c, y, slot] if only is None else full.at[c, y, slot, only]
        send(ref, ref, g_recv.at[slot, only or 0], device, s)

    def g_arrived(slot, only=None):
        receive(full.at[c, y, slot] if only is None else full.at[c, y, slot, only], g_recv.at[slot, only or 0])

    def g_spread(slot):
        ref = full.at[c, y, slot, 1]
        send(ref, ref, gy_recv.at[slot], at_y)
        send(ref, ref, one_recv.at[5], at_pair)

    def g_from_y(slot):
        ref = full.at[c, oy, slot, 1]
        receive(ref, gy_recv.at[slot])
        send(ref, ref, one_recv.at[5], at_pair)

    def g_from_x():
        g_arrived(jx)
        g_send(jx, (i, mine[0]), 1)
        g_send(jx, (i, mine[1]), 1)
        pl.when(mid)(lambda: g_send(jx, (i, mine[2]), 1, 1))
        g_spread(jx)

    def g_from_z(n):
        g_arrived(mine[n])
        if n == nz - 2:
            pl.when(mid)(lambda: g_send(mine[n], (i, edge * SIDE + x), None, 1))
        g_send(mine[n], at_x, 0)
        g_spread(mine[n])

    def g_from_far(n):
        g_arrived(far[n], 1)
        if n == nz - 2:
            pl.when(mid)(lambda: g_send(far[n], (i, edge * SIDE + x), 1, 1))
        g_spread(far[n])

    g_send(j, at_x)
    g_send(j, (i, mine[0]))
    g_send(j, (i, mine[1]))
    pl.when(mid)(lambda: g_send(j, (i, mine[2]), None, 1))
    g_spread(j)
    from_z(2, y)
    from_z(2, oy)

    def chunk_z(n, order=(0, 1)):
        chunk(pl.ds(zs[n] * SIDE, SIDE), order)

    def far_arrived(n):
        arrived(far[n], y)
        arrived(far[n], oy)

    far_arrived(0)
    chunk_z(0)
    g_from_x()
    g_from_z(0)
    far_arrived(1)
    chunk_z(1)
    g_from_z(1)
    g_from_far(0)
    receive(src.at[c, oy], one_recv.at[3])
    send(src.at[c, oy], src.at[c, oy], one_recv.at[4], at_pair)
    g_from_y(j)
    g_from_z(2)
    far_arrived(2)
    chunk_z(2, (1,))

    def rounded(b, ref):
        for h in range(repeat):
            ref[:, h * HEAD_DIM:(h + 1) * HEAD_DIM] = (dqa[b, h * rows:(h + 1) * rows] * scale).astype(BF16)

    rounded(1, dqs)
    send(dqs, dq16.at[c], one_recv.at[6], at_pair)
    g_from_far(1)
    chunk_z(2, (0,))
    rounded(0, dq16.at[c])
    g_from_far(2)
    for slot in [jx, mine[0], mine[1], far[0]]:
        g_from_y(slot)
    take(weight_size, 7)
    receive(src.at[oc], one_recv.at[4])
    for a in range(CORES):
        for b in range(sp // CORES):
            src_t[a, b] = jnp.transpose(src[a, b])
    receive(dq16.at[oc], one_recv.at[6])
    dt_ref[...] = (dot(dq16[0], wq[0], NT) + dot(dq16[1], wq[1], NT)).astype(BF16)
    g_from_y(mine[2])
    g_from_y(far[1])
    for n in range(nz - 1):
        g_arrived(far[n], 0)
    ds_ref[...] = (
        dot(full[c, y, :, 0].reshape(-1, kw), wk[...], NT) + dot(full[c, y, :, 1].reshape(-1, kw), wv[...], NT)
    ).astype(BF16)
    g_from_y(far[2])
    receive(full.at[oc, :, :, 1], one_recv.at[5])
    dw = None
    for b in range(sp // CORES):
        for a in range(CORES):
            term = dot(src_t[a, b], full[a, b, :, 1].reshape(-1, kw))
            dw = term if dw is None else dw + term
    dw_ref[...] = dw

    def sent_all(s):
        ref = units.at[pl.ds(0, sent[s] // unit)]
        pltpu.make_async_remote_copy(
            src_ref=ref, dst_ref=ref, send_sem=send_sem.at[s], recv_sem=one_recv.at[0],
            device_id=at_pair, device_id_type=MESH,
        ).wait_send()

    sent_all(0)
    pl.when(mid)(lambda: sent_all(1))
    pltpu.make_async_remote_copy(
        src_ref=lsev.at[0], dst_ref=lsev.at[1], send_sem=send_sem.at[2], recv_sem=one_recv.at[1],
        device_id=at_pair, device_id_type=MESH,
    ).wait_send()


def settle(*refs):
    count = (len(refs) - 1) // 2
    sems = refs[-1]
    copies = [pltpu.make_async_copy(refs[n], refs[count + n], sems.at[n]) for n in range(count)]
    for copy in copies:
        copy.start()
    for copy in copies:
        copy.wait()


def settled(arrays):
    hbm = pl.BlockSpec(memory_space=pl.ANY)
    vmem = pl.BlockSpec(memory_space=pltpu.VMEM)
    return pl.pallas_call(
        settle,
        out_shape=tuple(jax.ShapeDtypeStruct(a.shape, a.dtype) for a in arrays),
        in_specs=[vmem] * len(arrays),
        out_specs=(hbm,) * len(arrays),
        scratch_shapes=[pltpu.SemaphoreType.DMA((len(arrays),))],
        compiler_params=pltpu.CompilerParams(vmem_limit_bytes=16 * 1024 * 1024),
    )(*arrays)


def fused(sp, tp, queries, attn_out, log_norm, cotangent, keys, values, source, w_query, w_key, w_value):
    rows, model = queries.shape
    width = w_value.shape[0]
    rs, kw = keys.shape
    vmem, hbm = pl.BlockSpec(memory_space=pltpu.VMEM), pl.BlockSpec(memory_space=pl.ANY)
    dma = pltpu.SemaphoreType.DMA
    stack = (rows * HEADS // KV_HEADS, HEAD_DIM)
    half = model // KV_HEADS
    ny = sp // CORES
    scratch = [
        ((2, tp, sp * rs, HEAD_DIM), BF16), ((2, KV_HEADS, rs, HEAD_DIM), BF16),
        ((3, KV_HEADS) + stack, BF16), ((3,) + stack, BF16),
        ((KV_HEADS, width, half), BF16), (w_key.shape, BF16), (w_value.shape, BF16),
        ((CORES, ny) + source.shape, BF16), ((CORES, ny) + source.shape[::-1], BF16),
        ((2, HEADS, rows), F32), ((2, stack[0], 128), F32), ((2, stack[0], 128), F32),
        ((2,) + stack, F32), ((KV_HEADS, rows, half), BF16), ((rows, half), BF16),
        ((2, sp * rs, HEAD_DIM), F32), ((sp, 2, rs, HEAD_DIM), BF16), ((3, 2, rs, HEAD_DIM), BF16),
        ((CORES, ny, tp, 2, rs, kw), BF16), ((640,) + UNIT, BF16),
    ]
    return settled(pl.pallas_call(
        functools.partial(kernel, sp, tp),
        out_shape=(
            pltpu.VMEM((rows, width), BF16),
            pltpu.VMEM((source.shape[0], width), BF16),
            pltpu.VMEM(w_value.shape, F32),
        ),
        in_specs=[hbm] * 10,
        out_specs=(vmem,) * 3,
        scratch_shapes=[pltpu.VMEM(s, t) for s, t in scratch] + [
            dma((8,)), dma((3,)), dma((tp, ny)), dma((tp, 2)), dma((tp,)), dma((7,)),
        ],
        compiler_params=pltpu.CompilerParams(
            collective_id=0, has_side_effects=True, vmem_limit_bytes=VMEM_BYTES
        ),
    )(log_norm.T, keys, values, queries, attn_out, cotangent, source, w_query, w_key, w_value))


def shards(sp, tp, *args):
    queries, keys, source = args[0], args[4], args[6]
    if sp == 2 * CORES and tp == 4 * SIDE and queries.shape[0] == 128 and sp * keys.shape[0] == 128 and source.shape[0] == 256:
        return fused(sp, tp, *args)
    return plain(*args)


def plain(queries, attn_out, log_norm, cotangent, keys, values, source, w_query, w_key, w_value):
    single_precision = jnp.float32
    repeat = HEADS // KV_HEADS
    score_scale = 1.0 / math.sqrt(HEAD_DIM)
    rows = queries.shape[0]
    near_keys, near_values = (
        lax.all_gather(keys, "sp", axis=0, tiled=True),
        lax.all_gather(values, "sp", axis=0, tiled=True),
    )
    span = near_keys.shape[0]
    query_tensor4 = queries.reshape(rows, KV_HEADS, repeat, HEAD_DIM)
    output_gradient4 = cotangent.reshape(rows, KV_HEADS, repeat, HEAD_DIM)
    out4 = attn_out.reshape(rows, KV_HEADS, repeat, HEAD_DIM)
    shared_key_heads = near_keys.reshape(span, KV_HEADS, HEAD_DIM)
    shared_value_heads = near_values.reshape(span, KV_HEADS, HEAD_DIM)
    delta = jnp.sum(
        output_gradient4.astype(single_precision) * out4.astype(single_precision), axis=3
    )
    delta = jnp.transpose(delta, (1, 2, 0))[..., None]
    lse = jnp.transpose(log_norm.reshape(rows, KV_HEADS, repeat), (1, 2, 0))[..., None]
    logit_scores = (
        jnp.einsum(
            "znjk,wnk->njzw",
            query_tensor4,
            shared_key_heads,
            preferred_element_type=single_precision,
        )
        * score_scale
    )
    probs = jnp.exp(logit_scores - lse)
    probabilities16 = probs.astype(jnp.bfloat16)
    prob_gradient = jnp.einsum(
        "znjk,wnk->njzw",
        output_gradient4,
        shared_value_heads,
        preferred_element_type=single_precision,
    )
    score_gradient = (probs * (prob_gradient - delta)).astype(jnp.bfloat16)
    query_gradient_piece = (
        jnp.einsum(
            "wohn,nwb->hwob",
            score_gradient,
            shared_key_heads,
            preferred_element_type=single_precision,
        )
        * score_scale
    )
    query_gradient_piece = query_gradient_piece.reshape(rows, -1)
    key_gradient_piece = (
        jnp.einsum(
            "nkjv,jnka->vna", score_gradient, query_tensor4, preferred_element_type=single_precision
        )
        * score_scale
    )
    value_gradient_piece = jnp.einsum(
        "nkjv,jnka->vna", probabilities16, output_gradient4, preferred_element_type=single_precision
    )
    own_keys, own_values = (
        lax.psum_scatter(
            key_gradient_piece.reshape(span, -1).astype(jnp.bfloat16),
            "sp",
            scatter_dimension=0,
            tiled=True,
        ).astype(jnp.float32),
        lax.psum_scatter(
            value_gradient_piece.reshape(span, -1).astype(jnp.bfloat16),
            "sp",
            scatter_dimension=0,
            tiled=True,
        ).astype(jnp.float32),
    )
    stacked = jnp.concatenate(
        [own_keys.astype(jnp.bfloat16), own_values.astype(jnp.bfloat16)], axis=1
    )
    group = lax.all_gather(stacked, "tp", axis=0, tiled=True)
    weights = jnp.concatenate([w_key, w_value], axis=1)
    d_source = lax.dot_general(
        group, weights, (((1,), (1,)), ((), ())), preferred_element_type=single_precision
    ).astype(jnp.bfloat16)
    kv_width = w_value.shape[1]
    weight_term = lax.dot_general(
        source,
        group[:, kv_width:],
        (((0,), (0,)), ((), ())),
        preferred_element_type=single_precision,
    )
    d_wvalue = lax.psum(weight_term.astype(jnp.bfloat16), "sp").astype(jnp.float32)
    dq16 = lax.psum(query_gradient_piece, "tp").astype(jnp.bfloat16)
    d_target = lax.dot_general(
        dq16, w_query, (((1,), (1,)), ((), ())), preferred_element_type=single_precision
    ).astype(jnp.bfloat16)
    return (d_target, d_source, d_wvalue)


def solution(mesh):
    body = functools.partial(shards, mesh.shape["sp"], mesh.shape["tp"])
    in_specs = (
        P("sp", None),
        P("sp", None),
        P("sp", None),
        P("sp", None),
        P(("sp", "tp"), None),
        P(("sp", "tp"), None),
        P("sp", "tp"),
        P("tp", None),
        P("tp", None),
        P("tp", None),
    )
    out_specs = (P("sp", "tp"), P("sp", "tp"), P("tp", None))
    return jax.shard_map(body, mesh=mesh, in_specs=in_specs, out_specs=out_specs, check_vma=False)
```

time: 44.1 us -> 37.5 us (0.85)
  the two profiles are of different devices: /device:TPU:0 before, /device:TPU:1 now
where the time goes in v2:
time: 37.5 us; the launch traced here: 37.4 us
  Pallas kernels  36.7 us (98%)
  between operations  0.64 us (2%)
    pallas_call x1, Pallas kernels, fused(): pl.pallas_call(functools.partial(kernel, sp, tp), out_shape=(pltpu.VMEM((...  35.7 us
    pallas_call x1, Pallas kernels, settled(): pl.pallas_call(settle, out_shape=tuple((jax.ShapeDtypeStruct(a.shape, a.d...  1.01 us

profile of v2, /device:TPU:1, one launch (start us, length us, event | category | flops | bytes accessed | tf_op | source)
XLA Modules:
  0.0 37.4 jit_solution(4172382582423449336)
XLA Ops:
  0.6 35.7 %shard_map.121 = (bf16[128,384]{1,0:T(8,128)(2,1)S(1)}, bf16[256,384]{1,0:T(8,128)(2,1)S(1)}, f32[384,512]{1,0:T(8,128)S(1)}) custom-call(f32[12,128]{1,0:T(8,128)} %bitcast.1, bf16[32,512]{1,0:T(8,128)(2,1)} %k_hbm.1, bf16[32,512]{1,0:T(8,128)(2,1)} %v_hbm.1, bf16[128,3072]{1,0:T(8,128)(2,1)} %q_hbm.1, bf16[128,3072]{1,0:T(8,128)(2,1)} %o_hbm.1, ...), custom_call_target="tpu_custom_call" | custom-call | tf_op jit(solution)/shard_map/pallas_call | solution.py:394
  36.4 1.0 %shard_map.122 = (bf16[128,384]{1,0:T(8,128)(2,1)}, bf16[256,384]{1,0:T(8,128)(2,1)}, f32[384,512]{1,0:T(8,128)}) custom-call(bf16[128,384]{1,0:T(8,128)(2,1)S(1)} %get-tuple-element.6.refs_0_, bf16[256,384]{1,0:T(8,128)(2,1)S(1)} %get-tuple-element.7.refs_1_, f32[384,512]{1,0:T(8,128)S(1)} %get-tuple-element.8.refs_2_), custom_call_target="tpu_custom_call" | custom-call | tf_op jit(solution)/shard_map/pallas_call | solution.py:365

commit v3 on v2

--- a/solution.py
+++ b/solution.py
@@ -29,7 +29,8 @@
 def kernel(
     sp, tp, lse_hbm, k_hbm, v_hbm, q_hbm, o_hbm, do_hbm, src_hbm, wq_hbm, wk_hbm, wv_hbm,
     dt_ref, ds_ref, dw_ref,
-    kv, kvs, att, attr, wq, wk, wv, src, src_t, lsev, lse, delta, dqa, dq16, dqs, acc, part, got, full, units,
+    kv, kvs, att, attr, wq, wk, wv, wqt, wkt, wvt, src, src_t, lsev, lse, delta, dqa, dq16, dqs, acc, prob,
+    part, got, dkf, dvf, units,
     load_sem, send_sem, kv_recv, g_recv, gy_recv, one_recv,
 ):
     rows = q_hbm.shape[0]
@@ -60,7 +61,7 @@
 
     def send(a, b, r, device, s=0):
         pltpu.make_async_remote_copy(
-            src_ref=a, dst_ref=b, send_sem=send_sem.at[s], recv_sem=r, device_id=device, device_id_type=MESH,
+            src_ref=a, dst_ref=b, send_sem=send_sem.at[s % 3], recv_sem=r, device_id=device, device_id_type=MESH,
         ).start()
         if s < 2:
             sent[s] += bytes_of(a)
@@ -114,9 +115,7 @@
     load(lse_hbm, lsev.at[0], 5)
     src_size = load(src_hbm, src.at[c, y], 6)
     weight_size = load(wk_hbm, wk, 7) + load(wv_hbm, wv, 7)
-    half = wq.shape[2]
-    for g in range(KV_HEADS):
-        weight_size += load(wq_hbm.at[:, pl.ds(g * half, half)], wq.at[g], 7)
+    weight_size += load(wq_hbm, wq, 7)
     take(kv_size, 0)
     pl.semaphore_wait(barrier, len(near) + 2 * mid.astype(jnp.int32))
 
@@ -137,7 +136,7 @@
     send(kvs.at[:, oc], kv.at[:, j, own], kv_recv.at[j, y], at_pair)
     for a in range(3):
         take(head_size, 1 + a)
-        send(att.at[a, oc], attr.at[a], one_recv.at[0], at_pair)
+        send(att.at[a, oc], attr.at[a], one_recv.at[0 if a < 2 else 7], at_pair)
     pltpu.make_async_copy(lse_hbm, lsev.at[0], load_sem.at[5]).wait()
     send(lsev.at[0], lsev.at[1], one_recv.at[1], at_pair, 2)
     take(own_size, 4)
@@ -145,16 +144,26 @@
     def block(b, a):
         return att[a, c] if b == 0 else attr[a]
 
-    def statistics(b):
+    def deltas(b):
         for h in range(repeat):
             at = pl.ds(h * rows, rows)
             do, o = (att[a, c, at] if b == 0 else attr[a, at] for a in (1, 2))
             d = jnp.sum(do.astype(F32) * o.astype(F32), axis=1, keepdims=True)
             delta[b, at] = jnp.broadcast_to(d, (rows, 128))
+
+    def norms(b):
+        for h in range(repeat):
             row = jnp.where(c == 0, lsev[b, h:h + 1, :], lsev[b, repeat + h:repeat + h + 1, :])
-            lse[b, at] = jnp.transpose(jnp.broadcast_to(row * log2e, (128, rows)))
-
-    statistics(0)
+            lse[b, pl.ds(h * rows, rows)] = jnp.transpose(jnp.broadcast_to(row * log2e, (128, rows)))
+
+    norms(0)
+    deltas(0)
+    take(weight_size, 7)
+    for n in range(repeat):
+        columns = slice(n * kw, (n + 1) * kw)
+        wqt[columns, :] = jnp.transpose(wq[:, columns])
+    wkt[...] = jnp.transpose(wk[...])
+    wvt[...] = jnp.transpose(wv[...])
 
     def piece(slot, h):
         return kv.at[:, slot, pl.ds(pl.multiple_of(h * (CORES * rs), CORES * rs), CORES * rs)]
@@ -168,49 +177,66 @@
     def from_z(n, h):
         arrived(mine[n], h)
         relay(mine[n], h, at_x)
-        if n == nz - 2:
-            pl.when(mid)(lambda: relay(mine[n], h, (i, edge * SIDE + x), 1))
+
+    def last_z(h, early):
+        def body():
+            arrived(mine[nz - 2], h)
+            if early:
+                relay(mine[nz - 2], h, (i, edge * SIDE + x), 1)
+            relay(mine[nz - 2], h, at_x, 0 if early else 3)
+
+        pl.when(mid if early else jnp.logical_not(mid))(body)
 
     receive(kv.at[:, j, theirs], kv_recv.at[j, y])
     arrived(j, oy)
-    relay(j, oy, at_x)
     relay(j, oy, (i, mine[0]))
     relay(j, oy, (i, mine[1]))
     pl.when(mid)(lambda: relay(j, oy, (i, mine[2]), 1))
     from_z(0, y)
-    receive(attr, one_recv.at[0])
+    receive(attr.at[pl.ds(0, 2)], one_recv.at[0])
     receive(lsev.at[1], one_recv.at[1])
-    statistics(1)
+    norms(1)
 
     def wide(a, n):
         return a if n == 1 else jnp.concatenate([a] * n, axis=1)
 
-    def grads(b, keys, values):
-        n = keys.shape[0] // 128
-        p = jnp.exp2(dot(block(b, 0), keys, NT) * (scale * log2e) - wide(lse[b], n))
+    def probs(b, keys):
+        return jnp.exp2(dot(block(b, 0), keys, NT) * (scale * log2e) - wide(lse[b], keys.shape[0] // 128))
+
+    def scores(b, p, values):
         dp = dot(block(b, 1), values, NT)
-        return p, (p * (dp - wide(delta[b], n))).astype(BF16)
-
-    def local(b):
+        return (p * (dp - wide(delta[b], values.shape[0] // 128))).astype(BF16)
+
+    def part_send(t, r):
+        for g in range(CORES):
+            to = oy * CORES + g
+            send(part.at[t, to], got.at[t, 1 + c], r, (to, j))
+        send(part.at[t, y * CORES + oc], got.at[t, 0], r, at_pair)
+
+    for b in range(2):
+        p = probs(b, kv[0, j])
+        prob[b] = p
+        dv = dot(p.astype(BF16), block(b, 1), TN)
+        if b == 0:
+            acc[1] = dv
+        else:
+            part[1] = (acc[1] + dv).astype(BF16).reshape(sp, rs, HEAD_DIM)
+    part_send(1, one_recv.at[2])
+    arrived(jx, y)
+    relay(jx, y, at_y)
+    last_z(y, True)
+    receive(attr.at[2], one_recv.at[7])
+    deltas(1)
+    for b in range(2):
         keys = kv[0, j]
-        p, ds = grads(b, keys, kv[1, j])
+        ds = scores(b, prob[b], kv[1, j])
         dk = dot(ds, block(b, 0), TN)
-        dv = dot(p.astype(BF16), block(b, 1), TN)
         dqa[b] = dot(ds, keys)
         if b == 0:
             acc[0] = dk
-            acc[1] = dv
         else:
-            part[:, 0] = ((acc[0] + dk) * scale).astype(BF16).reshape(sp, rs, HEAD_DIM)
-            part[:, 1] = (acc[1] + dv).astype(BF16).reshape(sp, rs, HEAD_DIM)
-
-    local(0)
-    from_z(1, y)
-    local(1)
-    for g in range(CORES):
-        to = oy * CORES + g
-        send(part.at[to], got.at[1 + c], one_recv.at[2], (to, j))
-    send(part.at[y * CORES + oc], got.at[0], one_recv.at[2], at_pair)
+            part[0] = ((acc[0] + dk) * scale).astype(BF16).reshape(sp, rs, HEAD_DIM)
+    part_send(0, one_recv.at[8])
     take(src_size, 6)
     for device, r in ((at_y, 3), (at_pair, 4)):
         send(src.at[c, y], src.at[c, y], one_recv.at[r], device)
@@ -218,64 +244,67 @@
     def chunk(slots, order=(0, 1)):
         for b in order:
             keys, values = (kv[t, slots].reshape(-1, HEAD_DIM) for t in range(2))
-            _, ds = grads(b, keys, values)
-            dqa[b] += dot(ds, keys)
-
-    arrived(jx, y)
-    arrived(jx, oy)
-    chunk(pl.ds(jx, 1))
-    from_z(0, oy)
-    from_z(1, oy)
-    receive(got, one_recv.at[2])
-    here = part[i].astype(F32) + got[1 + c].astype(F32)
-    there = got[0].astype(F32) + got[1 + oc].astype(F32)
-    for g in range(KV_HEADS):
-        full[c, y, j, :, :, g * HEAD_DIM:(g + 1) * HEAD_DIM] = jnp.where(c == g, here, there).astype(BF16)
-
-    def g_send(slot, device, only=None, s=0):
-        ref = full.at[c, y, slot] if only is None else full.at[c, y, slot, only]
-        send(ref, ref, g_recv.at[slot, only or 0], device, s)
-
-    def g_arrived(slot, only=None):
-        receive(full.at[c, y, slot] if only is None else full.at[c, y, slot, only], g_recv.at[slot, only or 0])
-
-    def g_spread(slot):
-        ref = full.at[c, y, slot, 1]
-        send(ref, ref, gy_recv.at[slot], at_y)
-        send(ref, ref, one_recv.at[5], at_pair)
-
-    def g_from_y(slot):
-        ref = full.at[c, oy, slot, 1]
+            dqa[b] += dot(scores(b, probs(b, keys), values), keys)
+
+    def total(t):
+        here = part[t, i].astype(F32) + got[t, 1 + c].astype(F32)
+        there = got[t, 0].astype(F32) + got[t, 1 + oc].astype(F32)
+        ref = dkf.at[j] if t == 0 else dvf.at[c, y, j]
+        for g in range(KV_HEADS):
+            ref[:, g * HEAD_DIM:(g + 1) * HEAD_DIM] = jnp.where(c == g, here, there).astype(BF16)
+
+    def grad(t, slot):
+        return dkf.at[slot] if t == 0 else dvf.at[c, y, slot]
+
+    def g_send(t, slot, device, s=0):
+        send(grad(t, slot), grad(t, slot), g_recv.at[slot, t], device, s)
+
+    def g_arrived(t, slot):
+        receive(grad(t, slot), g_recv.at[slot, t])
+
+    def g_along_z(t, slot):
+        g_send(t, slot, (i, mine[0]))
+        g_send(t, slot, (i, mine[1]))
+        pl.when(mid)(lambda: g_send(t, slot, (i, mine[2]), 1))
+
+    def g_spread(slot, last=False, s=0):
+        ref = grad(1, slot)
+        send(ref, ref, gy_recv.at[slot], at_y, s)
+        send(ref, ref, one_recv.at[5], at_pair, s)
+        if last:
+            send(ref, ref, one_recv.at[5], (oy * CORES + oc, j), s)
+
+    def g_from_y(slot, last=False):
+        ref = dvf.at[c, oy, slot]
         receive(ref, gy_recv.at[slot])
-        send(ref, ref, one_recv.at[5], at_pair)
-
-    def g_from_x():
-        g_arrived(jx)
-        g_send(jx, (i, mine[0]), 1)
-        g_send(jx, (i, mine[1]), 1)
-        pl.when(mid)(lambda: g_send(jx, (i, mine[2]), 1, 1))
-        g_spread(jx)
-
-    def g_from_z(n):
-        g_arrived(mine[n])
-        if n == nz - 2:
-            pl.when(mid)(lambda: g_send(mine[n], (i, edge * SIDE + x), None, 1))
-        g_send(mine[n], at_x, 0)
-        g_spread(mine[n])
-
-    def g_from_far(n):
-        g_arrived(far[n], 1)
-        if n == nz - 2:
-            pl.when(mid)(lambda: g_send(far[n], (i, edge * SIDE + x), 1, 1))
-        g_spread(far[n])
-
-    g_send(j, at_x)
-    g_send(j, (i, mine[0]))
-    g_send(j, (i, mine[1]))
-    pl.when(mid)(lambda: g_send(j, (i, mine[2]), None, 1))
-    g_spread(j)
-    from_z(2, y)
-    from_z(2, oy)
+        if not last:
+            send(ref, ref, one_recv.at[5], at_pair)
+
+    def dv_from(slot):
+        g_arrived(1, slot)
+        g_spread(slot)
+
+    def dv_last(slot, early, last=False):
+        def body():
+            g_arrived(1, slot)
+            if early:
+                g_send(1, slot, (i, edge * SIDE + x), 1)
+            g_spread(slot, last, 0 if early else 3)
+
+        pl.when(mid if early else jnp.logical_not(mid))(body)
+
+    def dk_from(n):
+        g_arrived(0, mine[n])
+        g_send(0, mine[n], at_x)
+
+    def dk_last(early):
+        def body():
+            g_arrived(0, mine[nz - 2])
+            if early:
+                g_send(0, mine[nz - 2], (i, edge * SIDE + x), 1)
+            g_send(0, mine[nz - 2], at_x, 0 if early else 3)
+
+        pl.when(mid if early else jnp.logical_not(mid))(body)
 
     def chunk_z(n, order=(0, 1)):
         chunk(pl.ds(zs[n] * SIDE, SIDE), order)
@@ -284,18 +313,44 @@
         arrived(far[n], y)
         arrived(far[n], oy)
 
+    from_z(1, y)
+    receive(got.at[1], one_recv.at[2])
+    total(1)
+    g_send(1, j, at_x)
+    g_along_z(1, j)
+    g_spread(j)
+    from_z(0, oy)
+    last_z(oy, True)
+    arrived(jx, oy)
+    chunk(pl.ds(jx, 1))
+    receive(got.at[0], one_recv.at[8])
+    total(0)
+    g_along_z(0, j)
+    g_send(0, j, at_x)
+    from_z(1, oy)
+    g_arrived(1, jx)
+    g_along_z(1, jx)
+    g_spread(jx)
+    dv_from(mine[0])
+    last_z(y, False)
+    last_z(oy, False)
+    dv_last(mine[2], True)
     far_arrived(0)
     chunk_z(0)
-    g_from_x()
-    g_from_z(0)
+    dv_from(mine[1])
+    dv_from(far[0])
+    dv_last(far[2], True, True)
     far_arrived(1)
     chunk_z(1)
-    g_from_z(1)
-    g_from_far(0)
+    dv_last(mine[2], False)
+    dv_from(far[1])
     receive(src.at[c, oy], one_recv.at[3])
     send(src.at[c, oy], src.at[c, oy], one_recv.at[4], at_pair)
+    dk_from(0)
+    dk_from(1)
     g_from_y(j)
-    g_from_z(2)
+    g_from_y(jx)
+    dk_last(True)
     far_arrived(2)
     chunk_z(2, (1,))
 
@@ -303,36 +358,35 @@
         for h in range(repeat):
             ref[:, h * HEAD_DIM:(h + 1) * HEAD_DIM] = (dqa[b, h * rows:(h + 1) * rows] * scale).astype(BF16)
 
+    half = dqs.shape[1]
     rounded(1, dqs)
-    send(dqs, dq16.at[c], one_recv.at[6], at_pair)
-    g_from_far(1)
+    send(dqs, dq16.at[:, pl.ds(pl.multiple_of(c * half, half), half)], one_recv.at[6], at_pair)
+    dv_last(far[2], False, True)
+    dk_last(False)
     chunk_z(2, (0,))
-    rounded(0, dq16.at[c])
-    g_from_far(2)
-    for slot in [jx, mine[0], mine[1], far[0]]:
+    for h in range(repeat):
+        at = pl.ds(pl.multiple_of(c * half + h * HEAD_DIM, HEAD_DIM), HEAD_DIM)
+        dq16[:, at] = (dqa[0, h * rows:(h + 1) * rows] * scale).astype(BF16)
+    for slot in [mine[0], mine[1], far[0], mine[2], far[1]]:
         g_from_y(slot)
-    take(weight_size, 7)
     receive(src.at[oc], one_recv.at[4])
-    for a in range(CORES):
-        for b in range(sp // CORES):
-            src_t[a, b] = jnp.transpose(src[a, b])
-    receive(dq16.at[oc], one_recv.at[6])
-    dt_ref[...] = (dot(dq16[0], wq[0], NT) + dot(dq16[1], wq[1], NT)).astype(BF16)
-    g_from_y(mine[2])
-    g_from_y(far[1])
-    for n in range(nz - 1):
-        g_arrived(far[n], 0)
-    ds_ref[...] = (
-        dot(full[c, y, :, 0].reshape(-1, kw), wk[...], NT) + dot(full[c, y, :, 1].reshape(-1, kw), wv[...], NT)
-    ).astype(BF16)
-    g_from_y(far[2])
-    receive(full.at[oc, :, :, 1], one_recv.at[5])
-    dw = None
+    deep = src.shape[2]
     for b in range(sp // CORES):
         for a in range(CORES):
-            term = dot(src_t[a, b], full[a, b, :, 1].reshape(-1, kw))
-            dw = term if dw is None else dw + term
-    dw_ref[...] = dw
+            n = b * CORES + a
+            src_t[:, n * deep:(n + 1) * deep] = jnp.transpose(src[a, b])
+    receive(dq16.at[:, pl.ds(pl.multiple_of(oc * half, half), half)], one_recv.at[6])
+    dt_ref[...] = dot(dq16[...], wqt[...]).astype(BF16)
+    g_arrived(0, jx)
+    for n in range(nz - 1):
+        g_arrived(0, far[n])
+    ds_ref[...] = (
+        dot(dkf[...].reshape(-1, kw), wkt[...]) + dot(dvf[c, y].reshape(-1, kw), wvt[...])
+    ).astype(BF16)
+    g_from_y(far[2], True)
+    receive(dvf.at[oc], one_recv.at[5])
+    dw_ref[...] = dot(src_t[...], jnp.concatenate(
+        [dvf[a, b].reshape(-1, kw) for b in range(sp // CORES) for a in range(CORES)], axis=0))
 
     def sent_all(s):
         ref = units.at[pl.ds(0, sent[s] // unit)]
@@ -384,12 +438,14 @@
     scratch = [
         ((2, tp, sp * rs, HEAD_DIM), BF16), ((2, KV_HEADS, rs, HEAD_DIM), BF16),
         ((3, KV_HEADS) + stack, BF16), ((3,) + stack, BF16),
-        ((KV_HEADS, width, half), BF16), (w_key.shape, BF16), (w_value.shape, BF16),
-        ((CORES, ny) + source.shape, BF16), ((CORES, ny) + source.shape[::-1], BF16),
+        (w_query.shape, BF16), (w_key.shape, BF16), (w_value.shape, BF16),
+        (w_query.shape[::-1], BF16), (w_key.shape[::-1], BF16), (w_value.shape[::-1], BF16),
+        ((CORES, ny) + source.shape, BF16), ((width, sp * source.shape[0]), BF16),
         ((2, HEADS, rows), F32), ((2, stack[0], 128), F32), ((2, stack[0], 128), F32),
-        ((2,) + stack, F32), ((KV_HEADS, rows, half), BF16), ((rows, half), BF16),
-        ((2, sp * rs, HEAD_DIM), F32), ((sp, 2, rs, HEAD_DIM), BF16), ((3, 2, rs, HEAD_DIM), BF16),
-        ((CORES, ny, tp, 2, rs, kw), BF16), ((640,) + UNIT, BF16),
+        ((2,) + stack, F32), ((rows, model), BF16), ((rows, half), BF16),
+        ((2, sp * rs, HEAD_DIM), F32), ((2, stack[0], sp * rs), F32),
+        ((2, sp, rs, HEAD_DIM), BF16), ((2, 3, rs, HEAD_DIM), BF16),
+        ((tp, rs, kw), BF16), ((CORES, ny, tp, rs, kw), BF16), ((640,) + UNIT, BF16),
     ]
     return settled(pl.pallas_call(
         functools.partial(kernel, sp, tp),
@@ -401,7 +457,7 @@
         in_specs=[hbm] * 10,
         out_specs=(vmem,) * 3,
         scratch_shapes=[pltpu.VMEM(s, t) for s, t in scratch] + [
-            dma((8,)), dma((3,)), dma((tp, ny)), dma((tp, 2)), dma((tp,)), dma((7,)),
+            dma((8,)), dma((3,)), dma((tp, ny)), dma((tp, 2)), dma((tp,)), dma((9,)),
         ],
         compiler_params=pltpu.CompilerParams(
             collective_id=0, has_side_effects=True, vmem_limit_bytes=VMEM_BYTES

time: 37.5 us -> 30.9 us (0.82)
  the two profiles are of different devices: /device:TPU:1 before, /device:TPU:0 now
where the time goes in v3:
time: 30.9 us; the launch traced here: 30.7 us
  Pallas kernels  30.1 us (97%)
  between operations  0.64 us (2%)
    pallas_call x1, Pallas kernels, fused(): pl.pallas_call(functools.partial(kernel, sp, tp), out_shape=(pltpu.VMEM((...  29.1 us
    pallas_call x1, Pallas kernels, settled(): pl.pallas_call(settle, out_shape=tuple((jax.ShapeDtypeStruct(a.shape, a.d...  1.01 us

profile of v3, /device:TPU:0, one launch (start us, length us, event | category | flops | bytes accessed | tf_op | source)
XLA Modules:
  0.0 30.7 jit_solution(15750751984276733299)
XLA Ops:
  0.6 29.1 %shard_map.121 = (bf16[128,384]{1,0:T(8,128)(2,1)S(1)}, bf16[256,384]{1,0:T(8,128)(2,1)S(1)}, f32[384,512]{1,0:T(8,128)S(1)}) custom-call(f32[12,128]{1,0:T(8,128)} %bitcast.1, bf16[32,512]{1,0:T(8,128)(2,1)} %k_hbm.1, bf16[32,512]{1,0:T(8,128)(2,1)} %v_hbm.1, bf16[128,3072]{1,0:T(8,128)(2,1)} %q_hbm.1, bf16[128,3072]{1,0:T(8,128)(2,1)} %o_hbm.1, ...), custom_call_target="tpu_custom_call" | custom-call | tf_op jit(solution)/shard_map/pallas_call | solution.py:450
  29.7 1.0 %shard_map.122 = (bf16[128,384]{1,0:T(8,128)(2,1)}, bf16[256,384]{1,0:T(8,128)(2,1)}, f32[384,512]{1,0:T(8,128)}) custom-call(bf16[128,384]{1,0:T(8,128)(2,1)S(1)} %get-tuple-element.6.refs_0_, bf16[256,384]{1,0:T(8,128)(2,1)S(1)} %get-tuple-element.7.refs_1_, f32[384,512]{1,0:T(8,128)S(1)} %get-tuple-element.8.refs_2_), custom_call_target="tpu_custom_call" | custom-call | tf_op jit(solution)/shard_map/pallas_call | solution.py:419

commit v4 on v3

--- a/solution.py
+++ b/solution.py
@@ -13,7 +13,7 @@
 HEAD_DIM = 256
 CORES = 2
 SIDE = 2
-VMEM_BYTES = 62 * 1024 * 1024
+VMEM_BYTES = 64880640
 UNIT = (16, 256)
 MESH = pl.DeviceIdType.MESH
 NT = (((1,), (1,)), ((), ()))
@@ -28,9 +28,9 @@
 
 def kernel(
     sp, tp, lse_hbm, k_hbm, v_hbm, q_hbm, o_hbm, do_hbm, src_hbm, wq_hbm, wk_hbm, wv_hbm,
-    dt_ref, ds_ref, dw_ref,
-    kv, kvs, att, attr, wq, wk, wv, wqt, wkt, wvt, src, src_t, lsev, lse, delta, dqa, dq16, dqs, acc, prob,
-    part, got, dkf, dvf, units,
+    dt_ref, ds_ref, src_t, dvf,
+    kv, kvs, att, attr, wq, wk, wv, wqt, wkt, wvt, src, lsev, lse, delta, dqa, dq16, dqs, acc, prob,
+    part, got, dkf, units,
     load_sem, send_sem, kv_recv, g_recv, gy_recv, one_recv,
 ):
     rows = q_hbm.shape[0]
@@ -124,7 +124,11 @@
         for g in range(CORES):
             send(kvs.at[:, g], kv.at[:, j, own], kv_recv.at[j, y], (y_to * CORES + g, slot), s)
 
-    raw(oy, j)
+    for t in range(2):
+        for g in range(CORES):
+            to = (oy * CORES + g, j)
+            send(kvs.at[t, g], kv.at[t, j, own], kv_recv.at[j, y] if t == 0 else one_recv.at[9], to)
+        send(kvs.at[t, oc], kv.at[t, j, own], kv_recv.at[j, y] if t == 0 else one_recv.at[10], at_pair)
     raw(y, jx)
     raw(y, mine[0])
     raw(y, mine[1])
@@ -133,13 +137,20 @@
     def _():
         raw(y, mine[2], 1)
 
-    send(kvs.at[:, oc], kv.at[:, j, own], kv_recv.at[j, y], at_pair)
+    def src_send(first):
+        ref = src.at[c, y, pl.ds(0, cut) if first else pl.ds(cut, src.shape[2] - cut)]
+        send(ref, ref, one_recv.at[3], at_y)
+
+    cut = src.shape[2] * 5 // 8
     for a in range(3):
         take(head_size, 1 + a)
         send(att.at[a, oc], attr.at[a], one_recv.at[0 if a < 2 else 7], at_pair)
     pltpu.make_async_copy(lse_hbm, lsev.at[0], load_sem.at[5]).wait()
     send(lsev.at[0], lsev.at[1], one_recv.at[1], at_pair, 2)
     take(own_size, 4)
+    take(src_size, 6)
+    src_send(True)
+    send(src.at[c, y], src.at[c, y], one_recv.at[4], at_pair)
 
     def block(b, a):
         return att[a, c] if b == 0 else attr[a]
@@ -174,25 +185,28 @@
     def relay(slot, h, device, s=0):
         send(piece(slot, h), piece(slot, h), kv_recv.at[slot, h], device, s)
 
-    def from_z(n, h):
+    def from_z(n, h, s=0):
         arrived(mine[n], h)
-        relay(mine[n], h, at_x)
-
-    def last_z(h, early):
-        def body():
-            arrived(mine[nz - 2], h)
-            if early:
-                relay(mine[nz - 2], h, (i, edge * SIDE + x), 1)
-            relay(mine[nz - 2], h, at_x, 0 if early else 3)
-
-        pl.when(mid if early else jnp.logical_not(mid))(body)
-
-    receive(kv.at[:, j, theirs], kv_recv.at[j, y])
-    arrived(j, oy)
-    relay(j, oy, (i, mine[0]))
-    relay(j, oy, (i, mine[1]))
-    pl.when(mid)(lambda: relay(j, oy, (i, mine[2]), 1))
-    from_z(0, y)
+        relay(mine[n], h, at_x, s)
+
+    def half_piece(t):
+        return kv.at[t, j, pl.ds(pl.multiple_of(oy * (CORES * rs), CORES * rs), CORES * rs)]
+
+    def along_z(t):
+        def one(device, s=0):
+            send(half_piece(t), half_piece(t), kv_recv.at[j, oy], device, s)
+
+        one((i, mine[0]))
+        one(at_x)
+
+        @pl.when(mid)
+        def _():
+            one((i, mine[1]), 1)
+            one((i, mine[2]), 1)
+
+    receive(kv.at[0, j, theirs], kv_recv.at[j, y])
+    receive(half_piece(0), kv_recv.at[j, oy])
+    along_z(0)
     receive(attr.at[pl.ds(0, 2)], one_recv.at[0])
     receive(lsev.at[1], one_recv.at[1])
     norms(1)
@@ -222,9 +236,10 @@
         else:
             part[1] = (acc[1] + dv).astype(BF16).reshape(sp, rs, HEAD_DIM)
     part_send(1, one_recv.at[2])
-    arrived(jx, y)
-    relay(jx, y, at_y)
-    last_z(y, True)
+    receive(kv.at[1, j, theirs], one_recv.at[10])
+    receive(half_piece(1), one_recv.at[9])
+    along_z(1)
+    from_z(0, y)
     receive(attr.at[2], one_recv.at[7])
     deltas(1)
     for b in range(2):
@@ -234,12 +249,19 @@
         dqa[b] = dot(ds, keys)
         if b == 0:
             acc[0] = dk
+
+            @pl.when(mid)
+            def _():
+                arrived(mine[1], y)
+                relay(mine[1], y, at_x, 3)
+                arrived(mine[2], y)
+                relay(mine[2], y, (i, edge * SIDE + x), 1)
+                relay(mine[2], y, at_y, 3)
+
         else:
             part[0] = ((acc[0] + dk) * scale).astype(BF16).reshape(sp, rs, HEAD_DIM)
     part_send(0, one_recv.at[8])
-    take(src_size, 6)
-    for device, r in ((at_y, 3), (at_pair, 4)):
-        send(src.at[c, y], src.at[c, y], one_recv.at[r], device)
+    src_send(False)
 
     def chunk(slots, order=(0, 1)):
         for b in order:
@@ -265,7 +287,9 @@
     def g_along_z(t, slot):
         g_send(t, slot, (i, mine[0]))
         g_send(t, slot, (i, mine[1]))
-        pl.when(mid)(lambda: g_send(t, slot, (i, mine[2]), 1))
+        pl.when(mid)(lambda: g_send(t, slot, (i, mine[2]), 1 if t == 1 else 3))
+        if t == 0:
+            sent[0] += bytes_of(grad(t, slot))
 
     def g_spread(slot, last=False, s=0):
         ref = grad(1, slot)
@@ -297,15 +321,6 @@
         g_arrived(0, mine[n])
         g_send(0, mine[n], at_x)
 
-    def dk_last(early):
-        def body():
-            g_arrived(0, mine[nz - 2])
-            if early:
-                g_send(0, mine[nz - 2], (i, edge * SIDE + x), 1)
-            g_send(0, mine[nz - 2], at_x, 0 if early else 3)
-
-        pl.when(mid if early else jnp.logical_not(mid))(body)
-
     def chunk_z(n, order=(0, 1)):
         chunk(pl.ds(zs[n] * SIDE, SIDE), order)
 
@@ -313,44 +328,62 @@
         arrived(far[n], y)
         arrived(far[n], oy)
 
-    from_z(1, y)
     receive(got.at[1], one_recv.at[2])
     total(1)
     g_send(1, j, at_x)
     g_along_z(1, j)
     g_spread(j)
+
+    @pl.when(mid)
+    def _():
+        relay(mine[2], y, at_x, 3)
+
+    @pl.when(jnp.logical_not(mid))
+    def _():
+        arrived(mine[1], y)
+        relay(mine[1], y, at_x)
+
+    sent[0] += 2 * bytes_of(piece(mine[2], y))
     from_z(0, oy)
-    last_z(oy, True)
+    pl.when(mid)(lambda: from_z(2, oy, 3))
+    arrived(jx, y)
     arrived(jx, oy)
     chunk(pl.ds(jx, 1))
     receive(got.at[0], one_recv.at[8])
     total(0)
     g_along_z(0, j)
+    pl.when(jnp.logical_not(mid))(lambda: g_send(0, j, (i, mine[2]), 3))
     g_send(0, j, at_x)
     from_z(1, oy)
     g_arrived(1, jx)
     g_along_z(1, jx)
     g_spread(jx)
+
+    @pl.when(jnp.logical_not(mid))
+    def _():
+        arrived(mine[2], y)
+        relay(mine[2], y, at_y, 3)
+        relay(mine[2], y, at_x, 3)
+
     dv_from(mine[0])
-    last_z(y, False)
-    last_z(oy, False)
     dv_last(mine[2], True)
     far_arrived(0)
     chunk_z(0)
+    pl.when(jnp.logical_not(mid))(lambda: from_z(2, oy))
     dv_from(mine[1])
     dv_from(far[0])
     dv_last(far[2], True, True)
     far_arrived(1)
     chunk_z(1)
     dv_last(mine[2], False)
-    dv_from(far[1])
+    dk_from(0)
+    dk_from(1)
     receive(src.at[c, oy], one_recv.at[3])
     send(src.at[c, oy], src.at[c, oy], one_recv.at[4], at_pair)
-    dk_from(0)
-    dk_from(1)
     g_from_y(j)
     g_from_y(jx)
-    dk_last(True)
+    dv_from(far[1])
+    dk_from(2)
     far_arrived(2)
     chunk_z(2, (1,))
 
@@ -362,19 +395,18 @@
     rounded(1, dqs)
     send(dqs, dq16.at[:, pl.ds(pl.multiple_of(c * half, half), half)], one_recv.at[6], at_pair)
     dv_last(far[2], False, True)
-    dk_last(False)
     chunk_z(2, (0,))
     for h in range(repeat):
         at = pl.ds(pl.multiple_of(c * half + h * HEAD_DIM, HEAD_DIM), HEAD_DIM)
         dq16[:, at] = (dqa[0, h * rows:(h + 1) * rows] * scale).astype(BF16)
-    for slot in [mine[0], mine[1], far[0], mine[2], far[1]]:
-        g_from_y(slot)
     receive(src.at[oc], one_recv.at[4])
     deep = src.shape[2]
     for b in range(sp // CORES):
         for a in range(CORES):
             n = b * CORES + a
             src_t[:, n * deep:(n + 1) * deep] = jnp.transpose(src[a, b])
+    for slot in [mine[0], mine[1], far[0], mine[2], far[1]]:
+        g_from_y(slot)
     receive(dq16.at[:, pl.ds(pl.multiple_of(oc * half, half), half)], one_recv.at[6])
     dt_ref[...] = dot(dq16[...], wqt[...]).astype(BF16)
     g_arrived(0, jx)
@@ -385,8 +417,6 @@
     ).astype(BF16)
     g_from_y(far[2], True)
     receive(dvf.at[oc], one_recv.at[5])
-    dw_ref[...] = dot(src_t[...], jnp.concatenate(
-        [dvf[a, b].reshape(-1, kw) for b in range(sp // CORES) for a in range(CORES)], axis=0))
 
     def sent_all(s):
         ref = units.at[pl.ds(0, sent[s] // unit)]
@@ -403,27 +433,39 @@
     ).wait_send()
 
 
-def settle(*refs):
-    count = (len(refs) - 1) // 2
-    sems = refs[-1]
-    copies = [pltpu.make_async_copy(refs[n], refs[count + n], sems.at[n]) for n in range(count)]
-    for copy in copies:
+def finish(dt_ref, ds_ref, src_t, dvf, dt_hbm, ds_hbm, dw_hbm, dw_ref, sems):
+    small = [
+        pltpu.make_async_copy(a, b, sems.at[n]) for n, (a, b) in enumerate(((dt_ref, dt_hbm), (ds_ref, ds_hbm)))
+    ]
+    for copy in small:
         copy.start()
-    for copy in copies:
+    kw = dw_ref.shape[1]
+    dv = jnp.concatenate(
+        [dvf[a, b].reshape(-1, kw) for b in range(dvf.shape[1]) for a in range(CORES)], axis=0)
+    pieces = 3
+    tall = dw_ref.shape[0] // pieces
+    for n in range(pieces):
+        at = pl.ds(n * tall, tall)
+        dw_ref[at] = dot(src_t[at], dv)
+        copy = pltpu.make_async_copy(dw_ref.at[at], dw_hbm.at[at], sems.at[2 + n])
+        copy.start()
+        small.append(copy)
+    for copy in small:
         copy.wait()
 
 
-def settled(arrays):
-    hbm = pl.BlockSpec(memory_space=pl.ANY)
-    vmem = pl.BlockSpec(memory_space=pltpu.VMEM)
+def finished(shape, dt, ds, src_t, dvf):
+    vmem, hbm = pl.BlockSpec(memory_space=pltpu.VMEM), pl.BlockSpec(memory_space=pl.ANY)
     return pl.pallas_call(
-        settle,
-        out_shape=tuple(jax.ShapeDtypeStruct(a.shape, a.dtype) for a in arrays),
-        in_specs=[vmem] * len(arrays),
-        out_specs=(hbm,) * len(arrays),
-        scratch_shapes=[pltpu.SemaphoreType.DMA((len(arrays),))],
+        finish,
+        out_shape=(
+            jax.ShapeDtypeStruct(dt.shape, BF16), jax.ShapeDtypeStruct(ds.shape, BF16), jax.ShapeDtypeStruct(shape, F32),
+        ),
+        in_specs=[vmem] * 4,
+        out_specs=(hbm,) * 3,
+        scratch_shapes=[pltpu.VMEM(shape, F32), pltpu.SemaphoreType.DMA((5,))],
         compiler_params=pltpu.CompilerParams(vmem_limit_bytes=16 * 1024 * 1024),
-    )(*arrays)
+    )(dt, ds, src_t, dvf)
 
 
 def fused(sp, tp, queries, attn_out, log_norm, cotangent, keys, values, source, w_query, w_key, w_value):
@@ -440,24 +482,25 @@
         ((3, KV_HEADS) + stack, BF16), ((3,) + stack, BF16),
         (w_query.shape, BF16), (w_key.shape, BF16), (w_value.shape, BF16),
         (w_query.shape[::-1], BF16), (w_key.shape[::-1], BF16), (w_value.shape[::-1], BF16),
-        ((CORES, ny) + source.shape, BF16), ((width, sp * source.shape[0]), BF16),
+        ((CORES, ny) + source.shape, BF16),
         ((2, HEADS, rows), F32), ((2, stack[0], 128), F32), ((2, stack[0], 128), F32),
         ((2,) + stack, F32), ((rows, model), BF16), ((rows, half), BF16),
         ((2, sp * rs, HEAD_DIM), F32), ((2, stack[0], sp * rs), F32),
         ((2, sp, rs, HEAD_DIM), BF16), ((2, 3, rs, HEAD_DIM), BF16),
-        ((tp, rs, kw), BF16), ((CORES, ny, tp, rs, kw), BF16), ((640,) + UNIT, BF16),
+        ((tp, rs, kw), BF16), ((640,) + UNIT, BF16),
     ]
-    return settled(pl.pallas_call(
+    return finished(w_value.shape, *pl.pallas_call(
         functools.partial(kernel, sp, tp),
         out_shape=(
             pltpu.VMEM((rows, width), BF16),
             pltpu.VMEM((source.shape[0], width), BF16),
-            pltpu.VMEM(w_value.shape, F32),
+            pltpu.VMEM((width, sp * source.shape[0]), BF16),
+            pltpu.VMEM((CORES, ny, tp, rs, kw), BF16),
         ),
         in_specs=[hbm] * 10,
-        out_specs=(vmem,) * 3,
+        out_specs=(vmem,) * 4,
         scratch_shapes=[pltpu.VMEM(s, t) for s, t in scratch] + [
-            dma((8,)), dma((3,)), dma((tp, ny)), dma((tp, 2)), dma((tp,)), dma((9,)),
+            dma((8,)), dma((3,)), dma((tp, ny)), dma((tp, 2)), dma((tp,)), dma((11,)),
         ],
         compiler_params=pltpu.CompilerParams(
             collective_id=0, has_side_effects=True, vmem_limit_bytes=VMEM_BYTES

time: 30.9 us -> 29.9 us (0.968)
  Pallas kernels: 30.1 us -> 29.1 us
    pallas_call x1, Pallas kernels: 29.1 us -> 27.7 us  [fused(): pl.pallas_call(functools.partial(kernel, sp, tp), out_shape=(pltpu.VMEM((...]
    pallas_call x1, Pallas kernels: 1.01 us -> 1.34 us  [finished(): pl.pallas_call(finish, out_shape=(jax.ShapeDtypeStruct(dt.shape, BF16), j...]
where the time goes in v4:
time: 29.9 us; the launch traced here: 29.7 us
  Pallas kernels  29.1 us (97%)
  between operations  0.64 us (2%)
    pallas_call x1, Pallas kernels, fused(): pl.pallas_call(functools.partial(kernel, sp, tp), out_shape=(pltpu.VMEM((...  27.7 us
    pallas_call x1, Pallas kernels, finished(): pl.pallas_call(finish, out_shape=(jax.ShapeDtypeStruct(dt.shape, BF16), j...  1.34 us

profile of v4, /device:TPU:0, one launch (start us, length us, event | category | flops | bytes accessed | tf_op | source)
XLA Modules:
  0.0 29.7 jit_solution(17109413910708714954)
XLA Ops:
  0.6 27.7 %shard_map.121 = (bf16[128,384]{1,0:T(8,128)(2,1)S(1)}, bf16[256,384]{1,0:T(8,128)(2,1)S(1)}, bf16[384,1024]{1,0:T(8,128)(2,1)S(1)}, bf16[2,2,8,32,512]{4,3,2,1,0:T(8,128)(2,1)S(1)}) custom-call(f32[12,128]{1,0:T(8,128)} %bitcast.1, bf16[32,512]{1,0:T(8,128)(2,1)} %k_hbm.1, bf16[32,512]{1,0:T(8,128)(2,1)} %v_hbm.1, bf16[128,3072]{1,0:T(8,128)(2,1)} %q_hbm.1, ...), custom_call_target="tpu_custom_call" | custom-call | tf_op jit(solution)/shard_map/pallas_call | solution.py:492
  28.4 1.3 %shard_map.122 = (bf16[128,384]{1,0:T(8,128)(2,1)}, bf16[256,384]{1,0:T(8,128)(2,1)}, f32[384,512]{1,0:T(8,128)}) custom-call(bf16[128,384]{1,0:T(8,128)(2,1)S(1)} %get-tuple-element.7.dt_ref, bf16[256,384]{1,0:T(8,128)(2,1)S(1)} %get-tuple-element.8.ds_ref, bf16[384,1024]{1,0:T(8,128)(2,1)S(1)} %get-tuple-element.9.src_t, ...), custom_call_target="tpu_custom_call" | custom-call | tf_op jit(solution)/shard_map/pallas_call | solution.py:459

commit v5 on v4

--- a/solution.py
+++ b/solution.py
@@ -373,38 +373,38 @@
     dv_from(mine[1])
     dv_from(far[0])
     dv_last(far[2], True, True)
+    receive(src.at[c, oy], one_recv.at[3])
+    send(src.at[c, oy], src.at[c, oy], one_recv.at[4], at_pair)
     far_arrived(1)
     chunk_z(1)
     dv_last(mine[2], False)
     dk_from(0)
     dk_from(1)
-    receive(src.at[c, oy], one_recv.at[3])
-    send(src.at[c, oy], src.at[c, oy], one_recv.at[4], at_pair)
     g_from_y(j)
     g_from_y(jx)
     dv_from(far[1])
     dk_from(2)
-    far_arrived(2)
-    chunk_z(2, (1,))
-
-    def rounded(b, ref):
-        for h in range(repeat):
-            ref[:, h * HEAD_DIM:(h + 1) * HEAD_DIM] = (dqa[b, h * rows:(h + 1) * rows] * scale).astype(BF16)
-
-    half = dqs.shape[1]
-    rounded(1, dqs)
-    send(dqs, dq16.at[:, pl.ds(pl.multiple_of(c * half, half), half)], one_recv.at[6], at_pair)
-    dv_last(far[2], False, True)
-    chunk_z(2, (0,))
-    for h in range(repeat):
-        at = pl.ds(pl.multiple_of(c * half + h * HEAD_DIM, HEAD_DIM), HEAD_DIM)
-        dq16[:, at] = (dqa[0, h * rows:(h + 1) * rows] * scale).astype(BF16)
     receive(src.at[oc], one_recv.at[4])
     deep = src.shape[2]
     for b in range(sp // CORES):
         for a in range(CORES):
             n = b * CORES + a
             src_t[:, n * deep:(n + 1) * deep] = jnp.transpose(src[a, b])
+    far_arrived(2)
+    dv_last(far[2], False, True)
+    chunk_z(2, (1,))
+
+    def rounded(b, ref):
+        for h in range(repeat):
+            ref[:, h * HEAD_DIM:(h + 1) * HEAD_DIM] = (dqa[b, h * rows:(h + 1) * rows] * scale).astype(BF16)
+
+    half = dqs.shape[1]
+    rounded(1, dqs)
+    send(dqs, dq16.at[:, pl.ds(pl.multiple_of(c * half, half), half)], one_recv.at[6], at_pair)
+    chunk_z(2, (0,))
+    for h in range(repeat):
+        at = pl.ds(pl.multiple_of(c * half + h * HEAD_DIM, HEAD_DIM), HEAD_DIM)
+        dq16[:, at] = (dqa[0, h * rows:(h + 1) * rows] * scale).astype(BF16)
     for slot in [mine[0], mine[1], far[0], mine[2], far[1]]:
         g_from_y(slot)
     receive(dq16.at[:, pl.ds(pl.multiple_of(oc * half, half), half)], one_recv.at[6])

time: 29.9 us -> 29.2 us (0.977)
  Pallas kernels: 29.1 us -> 28.4 us
    pallas_call x1, Pallas kernels: 27.7 us -> 27.1 us  [fused(): pl.pallas_call(functools.partial(kernel, sp, tp), out_shape=(pltpu.VMEM((...]
where the time goes in v5:
time: 29.2 us; the launch traced here: 29.1 us
  Pallas kernels  28.4 us (97%)
  between operations  0.64 us (2%)
    pallas_call x1, Pallas kernels, fused(): pl.pallas_call(functools.partial(kernel, sp, tp), out_shape=(pltpu.VMEM((...  27.1 us
    pallas_call x1, Pallas kernels, finished(): pl.pallas_call(finish, out_shape=(jax.ShapeDtypeStruct(dt.shape, BF16), j...  1.33 us

profile of v5, /device:TPU:0, one launch (start us, length us, event | category | flops | bytes accessed | tf_op | source)
XLA Modules:
  0.0 29.1 jit_solution(14061462281558190295)
XLA Ops:
  0.6 27.1 %shard_map.121 = (bf16[128,384]{1,0:T(8,128)(2,1)S(1)}, bf16[256,384]{1,0:T(8,128)(2,1)S(1)}, bf16[384,1024]{1,0:T(8,128)(2,1)S(1)}, bf16[2,2,8,32,512]{4,3,2,1,0:T(8,128)(2,1)S(1)}) custom-call(f32[12,128]{1,0:T(8,128)} %bitcast.1, bf16[32,512]{1,0:T(8,128)(2,1)} %k_hbm.1, bf16[32,512]{1,0:T(8,128)(2,1)} %v_hbm.1, bf16[128,3072]{1,0:T(8,128)(2,1)} %q_hbm.1, ...), custom_call_target="tpu_custom_call" | custom-call | tf_op jit(solution)/shard_map/pallas_call | solution.py:492
  27.8 1.3 %shard_map.122 = (bf16[128,384]{1,0:T(8,128)(2,1)}, bf16[256,384]{1,0:T(8,128)(2,1)}, f32[384,512]{1,0:T(8,128)}) custom-call(bf16[128,384]{1,0:T(8,128)(2,1)S(1)} %get-tuple-element.7.dt_ref, bf16[256,384]{1,0:T(8,128)(2,1)S(1)} %get-tuple-element.8.ds_ref, bf16[384,1024]{1,0:T(8,128)(2,1)S(1)} %get-tuple-element.9.src_t, ...), custom_call_target="tpu_custom_call" | custom-call | tf_op jit(solution)/shard_map/pallas_call | solution.py:459

commit v6 on v5

--- a/solution.py
+++ b/solution.py
@@ -285,9 +285,9 @@
         receive(grad(t, slot), g_recv.at[slot, t])
 
     def g_along_z(t, slot):
+        pl.when(mid)(lambda: g_send(t, slot, (i, mine[2]), 1 if t == 1 else 3))
+        g_send(t, slot, (i, mine[1]))
         g_send(t, slot, (i, mine[0]))
-        g_send(t, slot, (i, mine[1]))
-        pl.when(mid)(lambda: g_send(t, slot, (i, mine[2]), 1 if t == 1 else 3))
         if t == 0:
             sent[0] += bytes_of(grad(t, slot))
 

time: 29.2 us -> 28.9 us (0.990)
  Pallas kernels: 28.4 us -> 27.9 us
    pallas_call x1, Pallas kernels: 27.1 us -> 26.6 us  [fused(): pl.pallas_call(functools.partial(kernel, sp, tp), out_shape=(pltpu.VMEM((...]
where the time goes in v6:
time: 28.9 us; the launch traced here: 28.6 us
  Pallas kernels  27.9 us (97%)
  between operations  0.64 us (2%)
    pallas_call x1, Pallas kernels, fused(): pl.pallas_call(functools.partial(kernel, sp, tp), out_shape=(pltpu.VMEM((...  26.6 us
    pallas_call x1, Pallas kernels, finished(): pl.pallas_call(finish, out_shape=(jax.ShapeDtypeStruct(dt.shape, BF16), j...  1.34 us

profile of v6, /device:TPU:0, one launch (start us, length us, event | category | flops | bytes accessed | tf_op | source)
XLA Modules:
  0.0 28.6 jit_solution(17346533831290705405)
XLA Ops:
  0.6 26.6 %shard_map.121 = (bf16[128,384]{1,0:T(8,128)(2,1)S(1)}, bf16[256,384]{1,0:T(8,128)(2,1)S(1)}, bf16[384,1024]{1,0:T(8,128)(2,1)S(1)}, bf16[2,2,8,32,512]{4,3,2,1,0:T(8,128)(2,1)S(1)}) custom-call(f32[12,128]{1,0:T(8,128)} %bitcast.1, bf16[32,512]{1,0:T(8,128)(2,1)} %k_hbm.1, bf16[32,512]{1,0:T(8,128)(2,1)} %v_hbm.1, bf16[128,3072]{1,0:T(8,128)(2,1)} %q_hbm.1, ...), custom_call_target="tpu_custom_call" | custom-call | tf_op jit(solution)/shard_map/pallas_call | solution.py:492
  27.2 1.3 %shard_map.122 = (bf16[128,384]{1,0:T(8,128)(2,1)}, bf16[256,384]{1,0:T(8,128)(2,1)}, f32[384,512]{1,0:T(8,128)}) custom-call(bf16[128,384]{1,0:T(8,128)(2,1)S(1)} %get-tuple-element.7.dt_ref, bf16[256,384]{1,0:T(8,128)(2,1)S(1)} %get-tuple-element.8.ds_ref, bf16[384,1024]{1,0:T(8,128)(2,1)S(1)} %get-tuple-element.9.src_t, ...), custom_call_target="tpu_custom_call" | custom-call | tf_op jit(solution)/shard_map/pallas_call | solution.py:459
